TPU v7x, 32 devices: a whole 2x2x4 slice. The times are simulated.
32 devices in a mesh: sp: 8 (over z, core), tp: 4 (over y, x).
Axes of the slice: x: 2, y: 2, z: 4, core: 2. Of those that a mesh axis runs over, the one named last changes fastest.
Arguments:
- cotangent: bfloat16 [1024, 2048], P('sp'), may hold values from -6 to 6
- moe_input: bfloat16 [1024, 2048], P('sp'), may hold values from -6 to 6
- expert_ids: int32 [1024, 2], P('sp'), may hold values from 0 to 7, all different within a row; in each aligned block of 128 rows (0 to 127, 128 to 255, ...) at most 48 rows name the same one
- group_weight: float32 [1024], P('sp'), may hold values from 0.3 to 1
- expert_weight: float32 [1024, 2], P('sp'), may hold values from 0.1 to 0.9
- mixer_out: bfloat16 [1024, 512], P('sp', 'tp'), may hold values from -6 to 6
- queries: bfloat16 [256, 1024], P('tp', 'sp'), may hold values from -6 to 6
- key_vectors: bfloat16 [256, 1024], P('tp', 'sp'), may hold values from -6 to 6
- value_vectors: bfloat16 [512, 1024], P('tp', 'sp'), may hold values from -6 to 6
- decay_rates: float32 [4, 1024], P('tp', 'sp'), may hold values from 0 to 1, as said below
- proj_weight: bfloat16 [2048, 512], P(None, 'tp'), may hold values from -0.25 to 0.25
- gate_weight: bfloat16 [8, 2048, 2048], P('sp', None, 'tp'), may hold values from -0.125 to 0.125
- up_weight: bfloat16 [8, 2048, 2048], P('sp', None, 'tp'), may hold values from -0.125 to 0.125
- down_weight: bfloat16 [8, 2048, 2048], P('sp', 'tp'), may hold values from -0.125 to 0.125
Outputs:
- grad_gate: bfloat16 [8, 2048, 2048], P('sp', None, 'tp')
- grad_up: bfloat16 [8, 2048, 2048], P('sp', None, 'tp')
- grad_down: bfloat16 [8, 2048, 2048], P('sp', 'tp')
- grad_proj: float32 [2048, 512], P('sp', 'tp')
- grad_queries: float32 [256, 1024], P('tp', 'sp')
- grad_keys: float32 [256, 1024], P('tp', 'sp')
- grad_values: float32 [512, 1024], P('tp', 'sp')
Inputs may be any that keep to these rules, and one draw needn't show every extreme that they name: `expert_ids`: in the rows of one device no expert is named by more than 48 entries, a bound that some block reaches; the 2 experts of a row differ. `decay_rates`: Positive.
All inputs are finite; a program needn't handle non-finite values.
Results may differ from a plain program's by a relative error of at most 0.0058.
Values may be sent and summed in bfloat16 or wider, within the bound.
A program may use at most 64 MiB of HBM per device.

v0:
```python
import jax
import jax.numpy as jnp
from jax import lax
from jax.sharding import PartitionSpec as P


def carried_in(part, axis, combine, identity, reverse):
    count = lax.axis_size(axis)
    place = lax.axis_index(axis)
    ahead = count - 1 - place if reverse else place
    gathered = jax.tree.map(lambda a: lax.all_gather(a, axis), part)
    state = jax.tree.map(lambda a, e: jnp.zeros_like(a) + jnp.asarray(e, a.dtype), part, identity)

    def one(lap, state):
        source = count - 1 - lap if reverse else lap
        return combine(
            state, jax.tree.map(lambda a: lax.dynamic_index_in_dim(a, source, 0, False), gathered)
        )

    return lax.fori_loop(0, ahead, one, state)


def slot_table(block_ids, experts_all, capacity):
    flat_ids = block_ids.reshape(-1)
    expert_range = jnp.arange(experts_all, dtype=jnp.int32)
    onehot = (flat_ids[:, None] == expert_range[None, :]).astype(jnp.int32)
    before = jnp.cumsum(onehot, axis=0) - onehot
    rank_in = jnp.sum(before * onehot, axis=1)
    slot_ids = flat_ids * capacity + rank_in
    slot_range = jnp.arange(experts_all * capacity, dtype=jnp.int32)
    entry_numbers = jnp.arange(1, flat_ids.shape[0] + 1, dtype=jnp.int32)
    owners = (
        jnp.sum(
            jnp.where(slot_ids[None, :] == slot_range[:, None], entry_numbers[None, :], 0), axis=1
        )
        - 1
    )
    return (slot_ids, owners)


def pack_rows(cotangent, moe_input, group_weight, expert_weight, expert_ids, experts_all, capacity):
    slot_ids, owners = slot_table(expert_ids, experts_all, capacity)
    present = owners >= 0
    entry_ids = jnp.maximum(owners, 0)
    token_ids = entry_ids // expert_ids.shape[1]
    route_weight = (group_weight[:, None] * expert_weight).reshape(-1)
    row_scale = jnp.where(present, route_weight[entry_ids], 0.0)
    cot_rows = (cotangent[token_ids].astype(jnp.float32) * row_scale[:, None]).astype(jnp.bfloat16)
    inp_rows = jnp.where(present[:, None], moe_input[token_ids], jnp.zeros((), moe_input.dtype))
    return (cot_rows, inp_rows, slot_ids)


def expert_backward(cot_blocks, inp_blocks, gate_weight, up_weight, down_weight):
    gate_pre = jnp.einsum(
        "secd,edf->secf", inp_blocks, gate_weight, preferred_element_type=jnp.float32
    )
    up_pre = jnp.einsum("secd,edf->secf", inp_blocks, up_weight, preferred_element_type=jnp.float32)
    sigmoid_gate = jax.nn.sigmoid(gate_pre)
    hidden = (gate_pre * sigmoid_gate * up_pre).astype(jnp.bfloat16)
    grad_down = jnp.einsum(
        "secf,secd->efd", hidden, cot_blocks, preferred_element_type=jnp.float32
    ).astype(jnp.bfloat16)
    hidden_grad = jnp.einsum(
        "secd,efd->secf", cot_blocks, down_weight, preferred_element_type=jnp.float32
    )
    gate_grad = (
        hidden_grad * up_pre * sigmoid_gate * (1.0 + gate_pre * (1.0 - sigmoid_gate))
    ).astype(jnp.bfloat16)
    up_grad = (hidden_grad * gate_pre * sigmoid_gate).astype(jnp.bfloat16)
    grad_gate = jnp.einsum(
        "secd,secf->edf", inp_blocks, gate_grad, preferred_element_type=jnp.float32
    ).astype(jnp.bfloat16)
    grad_up = jnp.einsum(
        "secd,secf->edf", inp_blocks, up_grad, preferred_element_type=jnp.float32
    ).astype(jnp.bfloat16)
    partial_grad = jnp.einsum(
        "secf,edf->secd", gate_grad, gate_weight, preferred_element_type=jnp.float32
    )
    partial_grad = partial_grad + jnp.einsum(
        "secf,edf->secd", up_grad, up_weight, preferred_element_type=jnp.float32
    )
    return (grad_gate, grad_up, grad_down, partial_grad)


def combine_slots(returned, slot_ids, top_count):
    picked = returned[slot_ids].astype(jnp.float32)
    return jnp.sum(picked.reshape(-1, top_count, returned.shape[1]), axis=1)


def carry_combine(earlier, later):
    earlier_state, earlier_decay = earlier
    later_state, later_decay = later
    return (
        earlier_state * later_decay[:, None, None, None] + later_state,
        earlier_decay * later_decay,
    )


def retention_grads(queries, key_vectors, value_vectors, out_grad, decay_rates):
    exact_result = lax.Precision.HIGHEST
    heads_here = decay_rates.shape[0]
    length = decay_rates.shape[1]
    query_full = queries.astype(jnp.float32).reshape(heads_here, -1, length)
    key_full = key_vectors.astype(jnp.float32).reshape(heads_here, -1, length)
    value_full = value_vectors.astype(jnp.float32).reshape(heads_here, -1, length)
    output_gradient = out_grad.reshape(heads_here, -1, length)
    key_size = query_full.shape[1]
    value_size = value_full.shape[1]
    score_scale = key_size ** (-0.5)
    prefix = jnp.cumsum(decay_rates, axis=1)
    ending = prefix[:, -1:]
    mixing = jnp.exp(-jnp.abs(prefix[:, :, None] - prefix[:, None, :]))
    scores = (
        score_scale
        * jnp.einsum("hkt,hks->hts", query_full, key_full, precision=exact_result)
        * mixing
    )
    score_grad = (
        score_scale
        * jnp.einsum("hvt,hvs->hts", output_gradient, value_full, precision=exact_result)
        * mixing
    )
    query_grad = jnp.einsum("hks,hts->hkt", key_full, score_grad, precision=exact_result)
    key_grad = jnp.einsum("hkt,hts->hks", query_full, score_grad, precision=exact_result)
    value_grad = jnp.einsum("hvt,hts->hvs", output_gradient, scores, precision=exact_result)
    toward_end = jnp.exp(prefix - ending)
    from_start = jnp.exp(-prefix)

    def outgoing(weight_tensors):
        key_value = jnp.einsum(
            "nlq,nyq->nly",
            key_full * weight_tensors[:, None, :],
            value_full,
            precision=exact_result,
        )
        query_cot = jnp.einsum(
            "nlq,nyq->nly",
            query_full * weight_tensors[:, None, :],
            output_gradient,
            precision=exact_result,
        )
        return jnp.stack([key_value, query_cot], axis=1)

    decay_whole = jnp.exp(-ending[:, 0])
    identity_pair = (
        jnp.zeros((heads_here, 2, key_size, value_size), jnp.float32),
        jnp.ones((heads_here,), jnp.float32),
    )
    lower_source = carried_in(
        (outgoing(toward_end), decay_whole), "sp", carry_combine, identity_pair, False
    )[0]
    upper_source = carried_in(
        (outgoing(from_start), decay_whole), "sp", carry_combine, identity_pair, True
    )[0]
    low_weight = score_scale * from_start[:, None, :]
    high_weight = score_scale * toward_end[:, None, :]
    query_grad = query_grad + low_weight * jnp.einsum(
        "jsd,jms->jmd", output_gradient, lower_source[:, 0], precision=exact_result
    )
    query_grad = query_grad + high_weight * jnp.einsum(
        "jsd,jms->jmd", output_gradient, upper_source[:, 0], precision=exact_result
    )
    key_grad = key_grad + low_weight * jnp.einsum(
        "cdu,cgd->cgu", value_full, lower_source[:, 1], precision=exact_result
    )
    key_grad = key_grad + high_weight * jnp.einsum(
        "cdu,cgd->cgu", value_full, upper_source[:, 1], precision=exact_result
    )
    value_grad = value_grad + low_weight * jnp.einsum(
        "qnu,qnp->qpu", key_full, lower_source[:, 1], precision=exact_result
    )
    value_grad = value_grad + high_weight * jnp.einsum(
        "qnu,qnp->qpu", key_full, upper_source[:, 1], precision=exact_result
    )
    return (
        query_grad.reshape(heads_here * key_size, length),
        key_grad.reshape(heads_here * key_size, length),
        value_grad.reshape(heads_here * value_size, length),
    )


def on_device(
    cotangent,
    moe_input,
    expert_ids,
    group_weight,
    expert_weight,
    mixer_out,
    queries,
    key_vectors,
    value_vectors,
    decay_rates,
    proj_weight,
    gate_weight,
    up_weight,
    down_weight,
):
    sp_count = lax.axis_size("sp")
    tp_count = lax.axis_size("tp")
    local_experts = gate_weight.shape[0]
    experts_all = local_experts * sp_count
    rows_here = cotangent.shape[0]
    top_count = expert_ids.shape[1]
    capacity = 3 * top_count * rows_here // (2 * experts_all)
    model_width = cotangent.shape[1]
    slice_width = model_width // tp_count
    offset = lax.axis_index("tp") * slice_width
    cot_rows, inp_rows, slot_ids = pack_rows(
        cotangent, moe_input, group_weight, expert_weight, expert_ids, experts_all, capacity
    )
    got_cot, got_inp = (
        lax.all_to_all(cot_rows, "sp", split_axis=0, concat_axis=0, tiled=True),
        lax.all_to_all(inp_rows, "sp", split_axis=0, concat_axis=0, tiled=True),
    )
    block_shape = (sp_count, local_experts, capacity, model_width)
    grad_gate, grad_up, grad_down, partial_grad = expert_backward(
        got_cot.reshape(block_shape),
        got_inp.reshape(block_shape),
        gate_weight,
        up_weight,
        down_weight,
    )
    partial_grad = partial_grad.reshape(-1, model_width)
    shared = lax.psum_scatter(partial_grad, "tp", scatter_dimension=1, tiled=True).astype(
        jnp.bfloat16
    )
    returned = lax.all_to_all(shared, "sp", split_axis=0, concat_axis=0, tiled=True)
    moe_grad = combine_slots(returned, slot_ids, top_count)
    cot_slice = lax.dynamic_slice_in_dim(cotangent, offset, slice_width, 1)
    resid_part = (cot_slice.astype(jnp.float32) + moe_grad).astype(jnp.bfloat16)
    resid_grad = lax.all_gather(resid_part, "tp", axis=1, tiled=True)
    grad_proj = lax.psum_scatter(
        lax.dot_general(
            resid_grad, mixer_out, (((0,), (0,)), ((), ())), preferred_element_type=jnp.float32
        ),
        "sp",
        scatter_dimension=0,
        tiled=True,
    )
    out_grad = lax.dot_general(
        proj_weight, resid_grad, (((0,), (1,)), ((), ())), preferred_element_type=jnp.float32
    )
    grad_queries, grad_keys, grad_values = retention_grads(
        queries, key_vectors, value_vectors, out_grad, decay_rates
    )
    return (grad_gate, grad_up, grad_down, grad_proj, grad_queries, grad_keys, grad_values)


def solution(mesh):
    return jax.shard_map(
        on_device,
        mesh=mesh,
        in_specs=(
            P("sp", None),
            P("sp", None),
            P("sp", None),
            P("sp"),
            P("sp", None),
            P("sp", "tp"),
            P("tp", "sp"),
            P("tp", "sp"),
            P("tp", "sp"),
            P("tp", "sp"),
            P(None, "tp"),
            P("sp", None, "tp"),
            P("sp", None, "tp"),
            P("sp", "tp", None),
        ),
        out_specs=(
            P("sp", None, "tp"),
            P("sp", None, "tp"),
            P("sp", "tp", None),
            P("sp", "tp"),
            P("tp", "sp"),
            P("tp", "sp"),
            P("tp", "sp"),
        ),
        check_vma=False,
    )
```

profile of v0, /device:TPU:0, one launch (start us, length us, event | category | flops | bytes accessed | tf_op | source)
XLA Modules:
  0.0 272.7 jit_solution(15405495852779020573)
XLA Ops:
  9.7 6.2 %gather_fusion = bf16[384,2048]{1,0:T(8,128)(2,1)} fusion(bf16[128,2048]{1,0:T(8,128)(2,1)} %param.19, s32[1024]{0:T(1024)S(1)} %pad_clamp_fusion.2), kind=kCustom, calls=%fused_computation | custom fusion | bytes 3147264 | tf_op jit(solution)/shard_map/gather | solution.py:49
  18.6 6.5 %all-to-all-start = ((bf16[8,48,2048]{2,1,0:T(8,128)(2,1)}), bf16[8,48,2048]{2,1,0:T(8,128)(2,1)}, u32[]{:S(2)}, u32[]{:S(2)}) async-start(bf16[8,48,2048]{2,1,0:T(8,128)(2,1)} %broadcast_select_fusion), calls=%async_computation | async-start | bytes 3145728 | tf_op jit(solution)/shard_map/all_to_all | solution.py:213
  25.1 3.1 %gather_fusion.1 = bf16[384,2048]{1,0:T(8,128)(2,1)} fusion(bf16[128,2048]{1,0:T(8,128)(2,1)S(1)} %copy-done.1, s32[1024]{0:T(1024)S(1)} %pad_clamp_fusion.2), kind=kCustom, calls=%fused_computation.1 | custom fusion | bytes 3147264 | tf_op jit(solution)/shard_map/gather | solution.py:48
  28.5 2.8 %gather_fusion.2 = f32[384]{0:T(512)S(1)} fusion(f32[256]{0:T(256)S(1)} %reshape.410, s32[1024]{0:T(1024)S(1)} %pad_clamp_fusion.1), kind=kCustom, calls=%fused_computation.2 | custom fusion | bytes 4608 | tf_op jit(solution)/shard_map/gather | solution.py:47
  31.4 2.9 %fusion = bf16[8,48,2048]{2,1,0:T(8,128)(2,1)} fusion(bf16[8,48,2048]{2,1,0:T(8,128)(2,1)} %bitcast.186, f32[8,48]{1,0:T(8,128)S(1)} %broadcast_select_fusion.1), kind=kLoop, calls=%fused_computation.12 | loop fusion | flops 2359296 | bytes 3147264 | tf_op jit(solution)/shard_map/convert_element_type | solution.py:48
  34.2 28.7 %all-to-all-done = bf16[8,48,2048]{2,1,0:T(8,128)(2,1)} async-done(((bf16[8,48,2048]{2,1,0:T(8,128)(2,1)}), bf16[8,48,2048]{2,1,0:T(8,128)(2,1)}, u32[]{:S(2)}, u32[]{:S(2)}) %all-to-all-start) | async-done | bytes 1572896 | tf_op jit(solution)/shard_map/all_to_all | solution.py:213
  62.9 4.3 %all-to-all-start.1 = ((bf16[8,48,2048]{2,1,0:T(8,128)(2,1)}), bf16[8,48,2048]{2,1,0:T(8,128)(2,1)}, u32[]{:S(2)}, u32[]{:S(2)}) async-start(bf16[8,48,2048]{2,1,0:T(8,128)(2,1)} %fusion), calls=%async_computation.1 | async-start | bytes 3145728 | tf_op jit(solution)/shard_map/all_to_all | solution.py:212
  67.3 3.9 %fusion.16 = f32[8,1,48,512]{3,2,0,1:T(8,128)} fusion(bf16[8,48,2048]{2,1,0:T(8,128)(2,1)} %all-to-all-done, bf16[1,2048,512]{2,1,0:T(8,128)(2,1)} %param.30), kind=kOutput, calls=%fused_computation.28 | convolution fusion | flops 805306368 | bytes 4456448 | tf_op jit(solution)/shard_map/secd,edf->secf/dot_general | solution.py:57
  71.2 3.3 %fusion.19 = f32[8,1,48,512]{3,2,0,1:T(8,128)} fusion(bf16[8,48,2048]{2,1,0:T(8,128)(2,1)} %all-to-all-done, bf16[1,2048,512]{2,1,0:T(8,128)(2,1)S(1)} %copy-done), kind=kOutput, calls=%fused_computation.29 | convolution fusion | flops 805306368 | bytes 4456448 | tf_op jit(solution)/shard_map/secd,edf->secf/dot_general | solution.py:54
  74.5 30.6 %all-to-all-done.1 = bf16[8,48,2048]{2,1,0:T(8,128)(2,1)} async-done(((bf16[8,48,2048]{2,1,0:T(8,128)(2,1)}), bf16[8,48,2048]{2,1,0:T(8,128)(2,1)}, u32[]{:S(2)}, u32[]{:S(2)}) %all-to-all-start.1) | async-done | bytes 1572896 | tf_op jit(solution)/shard_map/all_to_all | solution.py:212
  105.1 3.7 %multiply_convert_fusion.1 = (bf16[8,1,48,512]{3,2,0,1:T(8,128)(2,1)S(1)}, bf16[8,1,48,512]{3,2,0,1:T(8,128)(2,1)S(1)}) fusion(f32[8,1,48,512]{3,2,0,1:T(8,128)} %fusion.19, f32[8,1,48,512]{3,2,0,1:T(8,128)} %fusion.16, bf16[8,48,2048]{2,1,0:T(8,128)(2,1)} %all-to-all-done.1, bf16[1,512,2048]{2,1,0:T(8,128)(2,1)} %param.31), kind=kOutput, calls=%fused_computation.53 | convolution fusion | flops 807862272 | bytes 6029312 | tf_op jit(solution)/shard_map/secd,efd->secf/dot_general | solution.py:63
  110.3 2.7 %convolution_add_fusion = f32[8,48,2048]{2,1,0:T(8,128)} fusion(f32[8,48,2048]{2,1,0:T(8,128)S(1)} %fusion.4, bf16[1,2048,512]{2,1,0:T(8,128)(2,1)S(1)} %copy-done.2, bf16[8,1,48,512]{3,2,0,1:T(8,128)(2,1)S(1)} %get-tuple-element.199), kind=kOutput, calls=%fused_computation.13 | convolution fusion | flops 806092800 | bytes 8781824 | tf_op jit(solution)/shard_map/secf,edf->secd/dot_general | solution.py:79
  116.6 15.1 %all-reduce = f32[8]{0:T(128)} all-reduce(f32[8]{0:T(128)S(1)} %bitcast_dynamic-update-slice_fusion), channel_id=1, replica_groups=mesh['sp'=8,'tp'=4] {'sp'}, use_global_device_ids=true, to_apply=%add | all-reduce | flops 8 | bytes 64
  135.1 4.0 %fusion.2 = bf16[1,2048,512]{2,1,0:T(8,128)(2,1)} fusion(bf16[8,48,2048]{2,1,0:T(8,128)(2,1)} %all-to-all-done, bf16[8,1,48,512]{3,2,0,1:T(8,128)(2,1)S(1)} %get-tuple-element.199), kind=kOutput, calls=%fused_computation.15 | convolution fusion | flops 806354944 | bytes 4063232 | tf_op jit(solution)/shard_map/secd,secf->edf/dot_general | solution.py:73
  139.1 17.0 %reduce-scatter.3.cloned.1.call-done = f32[384,512]{1,0:T(8,128)} async-done(((f32[384,2048]{1,0:T(8,128)}), f32[384,512]{1,0:T(8,128)}) %reduce-scatter.3.cloned.1.call-update) | async-done | bytes 786448 | tf_op jit(solution)/shard_map/reduce_scatter | solution.py:224
  158.0 4.6 %all-to-all-start.2 = ((bf16[8,48,512]{2,1,0:T(8,128)(2,1)}), bf16[8,48,512]{2,1,0:T(8,128)(2,1)S(1)}, u32[]{:S(2)}, u32[]{:S(2)}) async-start(bf16[8,48,512]{2,1,0:T(8,128)(2,1)} %bitcast.42), calls=%async_computation.3 | async-start | bytes 786432 | tf_op jit(solution)/shard_map/all_to_all | solution.py:227
  162.9 4.1 %fusion.1 = bf16[1,2048,512]{2,1,0:T(8,128)(2,1)} fusion(bf16[8,48,2048]{2,1,0:T(8,128)(2,1)} %all-to-all-done, bf16[8,1,48,512]{3,2,0,1:T(8,128)(2,1)S(1)} %get-tuple-element.200), kind=kOutput, calls=%fused_computation.14 | convolution fusion | flops 806354944 | bytes 4063232 | tf_op jit(solution)/shard_map/secd,secf->edf/dot_general | solution.py:70
  167.0 4.1 %fusion.3 = bf16[1,512,2048]{2,1,0:T(8,128)(2,1)} fusion(bf16[8,48,2048]{2,1,0:T(8,128)(2,1)} %all-to-all-done.1, f32[8,1,48,512]{3,2,0,1:T(8,128)S(1)} %copy-done.13, f32[8,1,48,512]{3,2,0,1:T(8,128)S(1)} %copy-done.14), kind=kOutput, calls=%fused_computation.16 | convolution fusion | flops 807534592 | bytes 5242880 | tf_op jit(solution)/shard_map/secf,secd->efd/dot_general | solution.py:60
  171.1 4.1 %all-to-all-done.2 = bf16[8,48,512]{2,1,0:T(8,128)(2,1)S(1)} async-done(((bf16[8,48,512]{2,1,0:T(8,128)(2,1)}), bf16[8,48,512]{2,1,0:T(8,128)(2,1)S(1)}, u32[]{:S(2)}, u32[]{:S(2)}) %all-to-all-start.2) | async-done | bytes 393248 | tf_op jit(solution)/shard_map/all_to_all | solution.py:227
  177.3 10.4 %all_gather.21 = bf16[128,2048]{1,0:T(8,128)(2,1)S(1)} all-gather(bf16[128,512]{1,0:T(8,128)(2,1)S(1)} %add_convert_fusion), channel_id=1, replica_groups=mesh['sp'=8,'tp'=4] {'tp'}, dimensions={1}, use_global_device_ids=true | all-gather | bytes 655360 | tf_op jit(solution)/shard_map/all_gather | solution.py:231
  190.8 14.8 %all-gather = f32[8,2,64,128]{3,2,1,0:T(8,128)S(1)} all-gather(f32[1,2,64,128]{3,2,1,0:T(8,128)S(1)} %pad_maximum_fusion), channel_id=2, replica_groups=mesh['sp'=8,'tp'=4] {'sp'}, dimensions={0}, use_global_device_ids=true | all-gather | bytes 589824 | tf_op jit(solution)/shard_map/all_gather | solution.py:11
  206.4 25.7 %all-gather.1 = f32[8,2,64,128]{3,2,1,0:T(8,128)S(1)} all-gather(f32[1,2,64,128]{3,2,1,0:T(8,128)S(1)} %pad_maximum_fusion.1), channel_id=3, replica_groups=mesh['sp'=8,'tp'=4] {'sp'}, dimensions={0}, use_global_device_ids=true | all-gather | bytes 589824 | tf_op jit(solution)/shard_map/all_gather | solution.py:11
  234.4 8.9 %while.27 = (s32[]{:T(128)}, f32[1,2,64,128]{3,2,1,0:T(8,128)S(1)}, s32[]{:T(128)}, f32[8,1]{0,1:T(1,128)S(1)}, f32[8,1,2,64,128]{4,3,2,1,0:T(8,128)S(1)}, /*index=5*/s32[]{:T(128)}, s32[]{:T(128)}, s32[]{:T(128)}, s32[]{:T(128)}) while((s32[]{:T(128)}, f32[1,2,64,128]{3,2,1,0:T(8,128)S(1)}, s32[]{:T(128)}, f32[8,1]{0,1:T(1,128)S(1)}, ...), condition=%wide.region_11.12_spmd, body=%wide.region_10.11_spmd.sunk | while | flops 32774 | bytes 196767 | solution.py:20
  246.7 19.2 %reduce-scatter.5.cloned.1.call-done = f32[256,128]{1,0:T(8,128)} async-done(((f32[2048,128]{1,0:T(8,128)}), f32[256,128]{1,0:T(8,128)}) %reduce-scatter.5.cloned.1.call-update) | async-done | bytes 131088 | tf_op jit(solution)/shard_map/reduce_scatter | solution.py:232
  (110 shorter events, 35.6 us)
Async XLA Ops:
  7.2 64.1 %copy-start = (bf16[1,2048,512]{2,1,0:T(8,128)(2,1)S(1)}, bf16[1,2048,512]{2,1,0:T(8,128)(2,1)}, u32[]{:S(2)}) copy-start(bf16[1,2048,512]{2,1,0:T(8,128)(2,1)} %param.29) | copy-start | bytes 6291460
  18.6 6.5 %copy-start.1 = (bf16[128,2048]{1,0:T(8,128)(2,1)S(1)}, bf16[128,2048]{1,0:T(8,128)(2,1)}, u32[]{:S(2)}) copy-start(bf16[128,2048]{1,0:T(8,128)(2,1)} %param.18) | copy-start | bytes 1572868
  18.6 44.4 %all-to-all-start = ((bf16[8,48,2048]{2,1,0:T(8,128)(2,1)}), bf16[8,48,2048]{2,1,0:T(8,128)(2,1)}, u32[]{:S(2)}, u32[]{:S(2)}) async-start(bf16[8,48,2048]{2,1,0:T(8,128)(2,1)} %broadcast_select_fusion), calls=%async_computation | async-start | bytes 3145728 | tf_op jit(solution)/shard_map/all_to_all | solution.py:213
  25.0 3.1 %copy-start.8 = (f32[128,2]{0,1:T(2,128)S(1)}, f32[128,2]{0,1:T(2,128)}, u32[]{:S(2)}) copy-start(f32[128,2]{0,1:T(2,128)} %param.22) | copy-start | bytes 3076
  25.1 3.1 %copy-start.9 = (f32[128]{0:T(128)S(1)}, f32[128]{0:T(128)}, u32[]{:S(2)}) copy-start(f32[128]{0:T(128)} %param.21) | copy-start | bytes 1540
  62.9 42.1 %all-to-all-start.1 = ((bf16[8,48,2048]{2,1,0:T(8,128)(2,1)}), bf16[8,48,2048]{2,1,0:T(8,128)(2,1)}, u32[]{:S(2)}, u32[]{:S(2)}) async-start(bf16[8,48,2048]{2,1,0:T(8,128)(2,1)} %fusion), calls=%async_computation.1 | async-start | bytes 3145728 | tf_op jit(solution)/shard_map/all_to_all | solution.py:212
  67.3 88.9 %reduce-scatter.3.cloned.1.call-start = ((), (), s32[]{:S(2)}) async-start(), calls=%async_computation.5 | async-start | bytes 3932160 | tf_op jit(solution)/shard_map/reduce_scatter | solution.py:224
  108.7 1.6 copy-start.2
  113.1 0.7 copy-start.10
  113.1 2.2 copy-start.12
  113.1 18.6 %copy-start.7 = (s32[128,2]{0,1:T(2,128)S(1)}, s32[128,2]{0,1:T(2,128)}, u32[]{:S(2)}) copy-start(s32[128,2]{0,1:T(2,128)} %param.20) | copy-start | bytes 3076
  113.1 19.6 %copy-start.3 = (bf16[128,128]{1,0:T(8,128)(2,1)S(1)}, bf16[128,128]{1,0:T(8,128)(2,1)}, u32[]{:S(2)}) copy-start(bf16[128,128]{1,0:T(8,128)(2,1)} %param.26) | copy-start | bytes 98308
  113.1 19.6 %copy-start.4 = (bf16[64,128]{1,0:T(8,128)(2,1)S(1)}, bf16[64,128]{1,0:T(8,128)(2,1)}, u32[]{:S(2)}) copy-start(bf16[64,128]{1,0:T(8,128)(2,1)} %param.25) | copy-start | bytes 49156
  113.1 21.2 %copy-start.5 = (bf16[64,128]{1,0:T(8,128)(2,1)S(1)}, bf16[64,128]{1,0:T(8,128)(2,1)}, u32[]{:S(2)}) copy-start(bf16[64,128]{1,0:T(8,128)(2,1)} %param.24) | copy-start | bytes 49156
  158.0 17.1 %all-to-all-start.2 = ((bf16[8,48,512]{2,1,0:T(8,128)(2,1)}), bf16[8,48,512]{2,1,0:T(8,128)(2,1)S(1)}, u32[]{:S(2)}, u32[]{:S(2)}) async-start(bf16[8,48,512]{2,1,0:T(8,128)(2,1)} %bitcast.42), calls=%async_computation.3 | async-start | bytes 786432 | tf_op jit(solution)/shard_map/all_to_all | solution.py:227
  162.6 103.2 %reduce-scatter.5.cloned.1.call-start = ((), (), s32[]{:S(2)}) async-start(), calls=%async_computation.6 | async-start | bytes 1179648 | tf_op jit(solution)/shard_map/reduce_scatter | solution.py:232
  162.9 4.2 %copy-start.13 = (f32[8,1,48,512]{3,2,0,1:T(8,128)S(1)}, f32[8,1,48,512]{3,2,0,1:T(8,128)}, u32[]{:S(2)}) copy-start(f32[8,1,48,512]{3,2,0,1:T(8,128)} %fusion.16) | copy-start | bytes 2359300
  162.9 4.2 %copy-start.14 = (f32[8,1,48,512]{3,2,0,1:T(8,128)S(1)}, f32[8,1,48,512]{3,2,0,1:T(8,128)}, u32[]{:S(2)}) copy-start(f32[8,1,48,512]{3,2,0,1:T(8,128)} %fusion.19) | copy-start | bytes 2359300
  205.6 28.8 %copy-start.11 = (f32[8,1]{0,1:T(1,128)S(1)}, f32[8,1]{0,1:T(1,128)}, u32[]{:S(2)}) copy-start(f32[8,1]{0,1:T(1,128)} %get-tuple-element.339) | copy-start | bytes 100
  232.1 13.2 %copy-start.6 = (f32[128,128]{1,0:T(8,128)S(1)}, f32[128,128]{1,0:T(8,128)}, u32[]{:S(2)}) copy-start(f32[128,128]{1,0:T(8,128)} %fusion.24) | copy-start | bytes 196612
Sparse Core Ops, SparseCore 0:
  113.3 42.8 reduce-scatter.2
  234.3 31.5 reduce-scatter.4
where the time goes:
time: 274 us; the launch traced here: 273 us
  waiting for transfers between devices  99.6 us (36%)
  blocking collectives  66 us (24%)
  matrix products  37 us (14%)
  local copies, waits for them, and re-layouts  22.9 us (8%)
  other arithmetic  16.2 us (6%)
  starting transfers between devices  15.7 us (6%)
  between operations  15.1 us (6%)
    all_gather x2, blocking collectives, carried_in(): gathered = jax.tree.map(lambda a: lax.all_gather(a, axis), part)  40.5 us
    all_to_all x1, waiting for transfers between devices, on_device(): lax.all_to_all(cot_rows, 'sp', split_axis=0, concat_axis=0, tiled=True)  30.6 us
    all_to_all x1, waiting for transfers between devices, on_device(): lax.all_to_all(inp_rows, 'sp', split_axis=0, concat_axis=0, tiled=True)  28.7 us
    reduce_scatter x1, waiting for transfers between devices, on_device(): lax.psum_scatter(lax.dot_general(resid_grad, mixer_out, (((0,), (0,)), ((...  19.2 us
    reduce_scatter x1, waiting for transfers between devices, on_device(): lax.psum_scatter(partial_grad, 'tp', scatter_dimension=1, tiled=True)  17 us
    unnamed x1, blocking collectives  15.1 us
    all_gather x1, blocking collectives, on_device(): resid_grad = lax.all_gather(resid_part, 'tp', axis=1, tiled=True)  10.4 us
    all_to_all x1, starting transfers between devices, on_device(): lax.all_to_all(inp_rows, 'sp', split_axis=0, concat_axis=0, tiled=True)  6.49 us
  transfers between devices with their start and end apart: 5, of which 5 were waited for; matrix products, arithmetic and copies ran while one was open for 17% of the time, Pallas kernels for 0%

commit v1 on v0

v1 whole, which is shorter than its diff:
```python
import functools

import jax
import jax.numpy as jnp
from jax import lax
from jax.experimental import pallas as pl
from jax.experimental.pallas import tpu as pltpu
from jax.sharding import PartitionSpec as P

MESH = pl.DeviceIdType.MESH
VMEM = pl.BlockSpec(memory_space=pltpu.VMEM)


def near_first(count):
    order = [0]
    for step in range(1, count // 2 + 1):
        order.append(step)
        if count - step != step:
            order.append(count - step)
    return order


def greet(sp_count, tp_count, sp_place, tp_place, along_tp):
    barrier = pltpu.get_barrier_semaphore()
    for k in range(1, sp_count):
        pl.semaphore_signal(
            barrier,
            inc=1,
            device_id={"sp": lax.rem(sp_place + k, sp_count), "tp": tp_place},
            device_id_type=MESH,
        )
    if along_tp:
        for m in range(1, tp_count):
            pl.semaphore_signal(
                barrier,
                inc=1,
                device_id={"sp": sp_place, "tp": lax.rem(tp_place + m, tp_count)},
                device_id_type=MESH,
            )
    pl.semaphore_wait(barrier, sp_count - 1 + (tp_count - 1 if along_tp else 0))


def remote(src, dst, send_sem, recv_sem, sp_place, tp_place):
    return pltpu.make_async_remote_copy(
        src_ref=src,
        dst_ref=dst,
        send_sem=send_sem,
        recv_sem=recv_sem,
        device_id={"sp": sp_place, "tp": tp_place},
        device_id_type=MESH,
    )


def state_side(here, there, count):
    return (here + count - there) // count


def dispatch_kernel(
    sp_count, tp_count, cot_src, inp_src, state, cot_full, inp_full, state_all,
    local_sem, send_one, recv_one, send_two, recv_two, send_state, recv_state,
):
    me = lax.axis_index("sp")
    q = lax.axis_index("tp")
    width = cot_src.shape[2]
    square = tp_count == 4
    order = near_first(sp_count)
    arrays = ((cot_src, cot_full), (inp_src, inp_full))

    def columns(full, block, place):
        return full.at[block, :, pl.ds(pl.multiple_of(place * width, width), width)]

    if square:
        across_x = (q // 2) * 2 + (1 - lax.rem(q, 2))
        across_y = (1 - q // 2) * 2 + lax.rem(q, 2)
        across_both = (1 - q // 2) * 2 + (1 - lax.rem(q, 2))
        peers = (across_x, across_y)
        origins = (across_x, across_y)
    else:
        peers = tuple(lax.rem(q + m, tp_count) for m in range(1, tp_count))
        origins = tuple(lax.rem(q + tp_count - m, tp_count) for m in range(1, tp_count))

    greet(sp_count, tp_count, me, q, True)
    waits = []
    own = []
    for a, (src, full) in enumerate(arrays):
        copy = pltpu.make_async_copy(src.at[me], columns(full, me, q), local_sem.at[a])
        copy.start()
        own.append(copy)
    own_state = pltpu.make_async_copy(state.at[0], state_all.at[me], local_sem.at[2])
    own_state.start()
    for k in order[1:]:
        there = lax.rem(me + k, sp_count)
        for a, (src, full) in enumerate(arrays):
            copy = remote(
                src.at[there], columns(full, me, q), send_one.at[a, k], recv_one.at[a, k], there, q
            )
            copy.start()
            waits.append(copy)
    for k in order[1:]:
        there = lax.rem(me + k, sp_count)
        copy = remote(
            state.at[state_side(me, there, sp_count)],
            state_all.at[me],
            send_state.at[k],
            recv_state.at[k],
            there,
            q,
        )
        copy.start()
        waits.append(copy)

    def forward(k):
        block = lax.rem(me + sp_count - k, sp_count)
        for a, (src, full) in enumerate(arrays):
            if k == 0:
                own[a].wait()
            else:
                remote(
                    src.at[block], columns(full, block, q), send_one.at[a, k], recv_one.at[a, k], me, q
                ).wait_recv()
            for m, peer in enumerate(peers):
                piece = columns(full, block, q)
                copy = remote(piece, piece, send_two.at[a, k, m], recv_two.at[a, k, m], me, peer)
                copy.start()
                waits.append(copy)

    def arrived(a, k, m, place):
        block = lax.rem(me + sp_count - k, sp_count)
        piece = columns(arrays[a][1], block, place)
        remote(piece, piece, send_two.at[a, k, m], recv_two.at[a, k, m], me, q).wait_recv()
        return piece

    def relay(k):
        for a in range(2):
            for m, place in enumerate(origins):
                piece = arrived(a, k, m, place)
                if square and m == a:
                    copy = remote(
                        piece, piece, send_two.at[a, k, 2], recv_two.at[a, k, 2], me, peers[1 - a]
                    )
                    copy.start()
                    waits.append(copy)

    for number, k in enumerate(order):
        forward(k)
        if number:
            relay(order[number - 1])
    relay(order[-1])
    if square:
        for k in order:
            for a in range(2):
                arrived(a, k, 2, across_both)
    for k in order[1:]:
        source = lax.rem(me + sp_count - k, sp_count)
        remote(
            state.at[0], state_all.at[source], send_state.at[k], recv_state.at[k], me, q
        ).wait_recv()
    own_state.wait()
    for copy in waits:
        copy.wait_send()


def dispatch(cot_src, inp_src, state, sp_count, tp_count):
    rows, width = cot_src.shape[1:]
    full = jax.ShapeDtypeStruct((sp_count, rows, width * tp_count), cot_src.dtype)
    dma = pltpu.SemaphoreType.DMA
    return pl.pallas_call(
        functools.partial(dispatch_kernel, sp_count, tp_count),
        out_shape=(full, full, jax.ShapeDtypeStruct((sp_count,) + state.shape[1:], state.dtype)),
        in_specs=[VMEM] * 3,
        out_specs=(VMEM,) * 3,
        scratch_shapes=[
            dma((3,)),
            dma((2, sp_count)),
            dma((2, sp_count)),
            dma((2, sp_count, tp_count - 1)),
            dma((2, sp_count, tp_count - 1)),
            dma((sp_count,)),
            dma((sp_count,)),
        ],
        compiler_params=pltpu.CompilerParams(collective_id=0, has_side_effects=True),
    )(cot_src, inp_src, state)


def return_kernel(
    sp_count, tp_count, part, select, cot, resid,
    summed_in, outgoing, returned, send_rs, recv_rs, send_back, recv_back, send_ag, recv_ag,
):
    me = lax.axis_index("sp")
    q = lax.axis_index("tp")
    width = cot.shape[1]
    order = near_first(sp_count)

    def columns(place):
        return pl.ds(pl.multiple_of(place * width, width), width)

    greet(sp_count, tp_count, me, q, True)
    waits = []
    far_first = order[::-1]
    for k in far_first:
        block = lax.rem(me + k, sp_count)
        for m in range(1, tp_count):
            peer = lax.rem(q + m, tp_count)
            copy = remote(
                part.at[block, :, columns(peer)],
                summed_in.at[m - 1, block],
                send_rs.at[k, m - 1],
                recv_rs.at[k, m - 1],
                me,
                peer,
            )
            copy.start()
            waits.append(copy)
    for k in far_first:
        block = lax.rem(me + k, sp_count)
        total = part[block, :, columns(q)].astype(jnp.float32)
        for m in range(1, tp_count):
            remote(
                part.at[block, :, columns(q)],
                summed_in.at[m - 1, block],
                send_rs.at[k, m - 1],
                recv_rs.at[k, m - 1],
                me,
                q,
            ).wait_recv()
            total = total + summed_in[m - 1, block].astype(jnp.float32)
        outgoing[block] = total.astype(outgoing.dtype)
        if k:
            copy = remote(
                outgoing.at[block], returned.at[me], send_back.at[k], recv_back.at[k], block, q
            )
            copy.start()
            waits.append(copy)
    total = jnp.dot(select[me], outgoing[me], preferred_element_type=jnp.float32)
    for k in far_first[:-1]:
        source = lax.rem(me + sp_count - k, sp_count)
        remote(
            outgoing.at[source], returned.at[source], send_back.at[k], recv_back.at[k], me, q
        ).wait_recv()
        total = total + jnp.dot(
            select[source], returned[source], preferred_element_type=jnp.float32
        )
    resid[:, columns(q)] = (cot[...].astype(jnp.float32) + total).astype(resid.dtype)
    for m in range(1, tp_count):
        piece = resid.at[:, columns(q)]
        copy = remote(
            piece, piece, send_ag.at[m - 1], recv_ag.at[m - 1], me, lax.rem(q + m, tp_count)
        )
        copy.start()
        waits.append(copy)
    for m in range(1, tp_count):
        piece = resid.at[:, columns(lax.rem(q + tp_count - m, tp_count))]
        remote(piece, piece, send_ag.at[m - 1], recv_ag.at[m - 1], me, q).wait_recv()
    for copy in waits:
        copy.wait_send()


def bring_back(part, select, cot_slice, sp_count, tp_count):
    rows = part.shape[1]
    tokens, width = cot_slice.shape
    dma = pltpu.SemaphoreType.DMA
    return pl.pallas_call(
        functools.partial(return_kernel, sp_count, tp_count),
        out_shape=jax.ShapeDtypeStruct((tokens, width * tp_count), cot_slice.dtype),
        in_specs=[VMEM] * 3,
        out_specs=VMEM,
        scratch_shapes=[
            pltpu.VMEM((tp_count - 1, sp_count, rows, width), part.dtype),
            pltpu.VMEM((sp_count, rows, width), part.dtype),
            pltpu.VMEM((sp_count, rows, width), part.dtype),
            dma((sp_count, tp_count - 1)),
            dma((sp_count, tp_count - 1)),
            dma((sp_count,)),
            dma((sp_count,)),
            dma((tp_count - 1,)),
            dma((tp_count - 1,)),
        ],
        compiler_params=pltpu.CompilerParams(collective_id=1, has_side_effects=True),
    )(part, select, cot_slice)


def share_kernel(
    sp_count, tp_count, state, proj, state_all, proj_all,
    local_sem, send_state, recv_state, send_proj, recv_proj,
):
    me = lax.axis_index("sp")
    q = lax.axis_index("tp")
    order = near_first(sp_count)[1:][::-1]
    greet(sp_count, tp_count, me, q, False)
    own_state = pltpu.make_async_copy(state.at[0], state_all.at[me], local_sem.at[0])
    own_proj = pltpu.make_async_copy(proj.at[me], proj_all.at[me], local_sem.at[1])
    own_state.start()
    own_proj.start()
    waits = []
    for k in order:
        there = lax.rem(me + k, sp_count)
        side = state_side(me, there, sp_count)
        for copy in (
            remote(state.at[side], state_all.at[me], send_state.at[k], recv_state.at[k], there, q),
            remote(proj.at[there], proj_all.at[me], send_proj.at[k], recv_proj.at[k], there, q),
        ):
            copy.start()
            waits.append(copy)
    own_state.wait()
    own_proj.wait()
    for k in order:
        source = lax.rem(me + sp_count - k, sp_count)
        remote(
            state.at[0], state_all.at[source], send_state.at[k], recv_state.at[k], me, q
        ).wait_recv()
        remote(
            proj.at[source], proj_all.at[source], send_proj.at[k], recv_proj.at[k], me, q
        ).wait_recv()
    for copy in waits:
        copy.wait_send()


def share(state, proj, sp_count, tp_count):
    dma = pltpu.SemaphoreType.DMA
    return pl.pallas_call(
        functools.partial(share_kernel, sp_count, tp_count),
        out_shape=(
            jax.ShapeDtypeStruct((sp_count,) + state.shape[1:], state.dtype),
            jax.ShapeDtypeStruct(proj.shape, proj.dtype),
        ),
        in_specs=[VMEM] * 2,
        out_specs=(VMEM,) * 2,
        scratch_shapes=[
            dma((2,)), dma((sp_count,)), dma((sp_count,)), dma((sp_count,)), dma((sp_count,)),
        ],
        compiler_params=pltpu.CompilerParams(collective_id=2, has_side_effects=True),
    )(state, proj)


def slot_numbers(ids, experts_all, capacity):
    rows, top_count = ids.shape
    onehot = ids[:, :, None] == jnp.arange(experts_all, dtype=jnp.int32)
    row_tally = jnp.sum(onehot.astype(jnp.float32), axis=1)
    place = jnp.arange(rows, dtype=jnp.int32)
    below = (place[:, None] > place[None, :]).astype(jnp.bfloat16)
    before = jnp.dot(below, row_tally.astype(jnp.bfloat16), preferred_element_type=jnp.float32)
    slots = []
    for j in range(top_count):
        here = onehot[:, j].astype(jnp.float32)
        rank = jnp.sum(here * before, axis=1).astype(jnp.int32)
        before = before + here
        slots.append(ids[:, j] * capacity + rank)
    return slots


def expert_forward(cot_blocks, inp_blocks, gate_weight, up_weight, down_weight):
    gate_pre = jnp.einsum(
        "secd,edf->secf", inp_blocks, gate_weight, preferred_element_type=jnp.float32
    )
    up_pre = jnp.einsum("secd,edf->secf", inp_blocks, up_weight, preferred_element_type=jnp.float32)
    sigmoid_gate = jax.nn.sigmoid(gate_pre)
    hidden = (gate_pre * sigmoid_gate * up_pre).astype(jnp.bfloat16)
    hidden_grad = jnp.einsum(
        "secd,efd->secf", cot_blocks, down_weight, preferred_element_type=jnp.float32
    )
    gate_grad = (
        hidden_grad * up_pre * sigmoid_gate * (1.0 + gate_pre * (1.0 - sigmoid_gate))
    ).astype(jnp.bfloat16)
    up_grad = (hidden_grad * gate_pre * sigmoid_gate).astype(jnp.bfloat16)
    partial_grad = jnp.einsum(
        "secf,edf->secd", gate_grad, gate_weight, preferred_element_type=jnp.float32
    )
    partial_grad = partial_grad + jnp.einsum(
        "secf,edf->secd", up_grad, up_weight, preferred_element_type=jnp.float32
    )
    return hidden, gate_grad, up_grad, partial_grad.astype(jnp.bfloat16)


def on_device(
    cotangent,
    moe_input,
    expert_ids,
    group_weight,
    expert_weight,
    mixer_out,
    queries,
    key_vectors,
    value_vectors,
    decay_rates,
    proj_weight,
    gate_weight,
    up_weight,
    down_weight,
):
    exact = lax.Precision.HIGHEST
    sp_count = lax.axis_size("sp")
    tp_count = lax.axis_size("tp")
    me = lax.axis_index("sp")
    local_experts = gate_weight.shape[0]
    experts_all = local_experts * sp_count
    rows_here, model_width = cotangent.shape
    top_count = expert_ids.shape[1]
    capacity = 3 * top_count * rows_here // (2 * experts_all)
    slice_width = model_width // tp_count
    offset = lax.axis_index("tp") * slice_width
    slot_count = experts_all * capacity

    slots = slot_numbers(expert_ids, experts_all, capacity)
    slot_range = jnp.arange(slot_count, dtype=jnp.int32)
    hits = [slot_range[:, None] == s[None, :] for s in slots]
    select = functools.reduce(jnp.logical_or, hits).astype(jnp.bfloat16)
    route = group_weight[:, None] * expert_weight
    row_scale = sum(
        jnp.sum(jnp.where(h, route[:, j][None, :], 0.0), axis=1) for j, h in enumerate(hits)
    )
    cot_slice = lax.dynamic_slice_in_dim(cotangent, offset, slice_width, 1)
    inp_slice = lax.dynamic_slice_in_dim(moe_input, offset, slice_width, 1)
    cot_rows = jnp.dot(select, cot_slice, preferred_element_type=jnp.float32)
    cot_rows = (cot_rows * row_scale[:, None]).astype(jnp.bfloat16)
    inp_rows = jnp.dot(select, inp_slice, preferred_element_type=jnp.float32).astype(jnp.bfloat16)
    block_rows = local_experts * capacity

    heads_here, length = decay_rates.shape
    query_full = queries.astype(jnp.float32).reshape(heads_here, -1, length)
    key_full = key_vectors.astype(jnp.float32).reshape(heads_here, -1, length)
    value_full = value_vectors.astype(jnp.float32).reshape(heads_here, -1, length)
    key_size = query_full.shape[1]
    value_size = value_full.shape[1]
    score_scale = key_size ** (-0.5)
    place = jnp.arange(length, dtype=jnp.int32)
    prefix = jnp.dot(
        decay_rates, (place[:, None] <= place[None, :]).astype(jnp.float32), precision=exact
    )
    ending = prefix[:, -1:]
    mixing = score_scale * jnp.exp(-jnp.abs(prefix[:, :, None] - prefix[:, None, :]))
    toward_end = jnp.exp(prefix - ending)
    from_start = jnp.exp(-prefix)
    both_weights = jnp.stack([toward_end, from_start])
    key_state = jnp.einsum(
        "whkl,hvl->whkv", key_full[None] * both_weights[:, :, None, :], value_full, precision=exact
    )
    totals_rows = jnp.broadcast_to(
        ending[None, :, :, None], (2, heads_here, 8, value_size)
    )
    key_state = jnp.concatenate([key_state, totals_rows], axis=2)

    got_cot, got_inp, key_states = dispatch(
        cot_rows.reshape(sp_count, block_rows, slice_width),
        inp_rows.reshape(sp_count, block_rows, slice_width),
        key_state,
        sp_count,
        tp_count,
    )
    block_shape = (sp_count, local_experts, capacity, model_width)
    cot_blocks = got_cot.reshape(block_shape)
    inp_blocks = got_inp.reshape(block_shape)
    hidden, gate_grad, up_grad, partial_grad = expert_forward(
        cot_blocks, inp_blocks, gate_weight, up_weight, down_weight
    )

    select_back = select.reshape(sp_count, block_rows, rows_here).transpose(0, 2, 1)
    resid_grad = bring_back(
        partial_grad.reshape(sp_count, block_rows, model_width),
        select_back,
        cot_slice,
        sp_count,
        tp_count,
    )
    grad_down = jnp.einsum(
        "secf,secd->efd", hidden, cot_blocks, preferred_element_type=jnp.float32
    ).astype(jnp.bfloat16)
    grad_gate = jnp.einsum(
        "secd,secf->edf", inp_blocks, gate_grad, preferred_element_type=jnp.float32
    ).astype(jnp.bfloat16)
    grad_up = jnp.einsum(
        "secd,secf->edf", inp_blocks, up_grad, preferred_element_type=jnp.float32
    ).astype(jnp.bfloat16)

    proj_part = lax.dot_general(
        resid_grad, mixer_out, (((0,), (0,)), ((), ())), preferred_element_type=jnp.float32
    ).astype(jnp.bfloat16)
    out_grad = lax.dot_general(
        proj_weight, resid_grad, (((0,), (1,)), ((), ())), preferred_element_type=jnp.float32
    ).reshape(heads_here, -1, length)
    query_state = jnp.einsum(
        "whkl,hvl->whkv", query_full[None] * both_weights[:, :, None, :], out_grad, precision=exact
    )
    query_states, proj_parts = share(
        query_state, proj_part.reshape(sp_count, model_width // sp_count, -1), sp_count, tp_count
    )
    grad_proj = jnp.sum(proj_parts.astype(jnp.float32), axis=0)

    totals = key_states[:, :, key_size, 0]
    block = jnp.arange(sp_count, dtype=jnp.int32)
    low_between = (block[None, :] > block[:, None]) & (block[None, :] < me)
    high_between = (block[None, :] < block[:, None]) & (block[None, :] > me)
    low_decay = jnp.exp(-jnp.sum(jnp.where(low_between[:, :, None], totals[None], 0.0), axis=1))
    high_decay = jnp.exp(-jnp.sum(jnp.where(high_between[:, :, None], totals[None], 0.0), axis=1))
    low_decay = jnp.where((block < me)[:, None], low_decay, 0.0)
    high_decay = jnp.where((block > me)[:, None], high_decay, 0.0)
    both_decays = jnp.stack([low_decay, high_decay])[:, :, :, None, None]
    key_carried = jnp.sum(both_decays * key_states[None, :, :, :key_size], axis=1)
    query_carried = jnp.sum(both_decays * query_states[None], axis=1)

    scores = mixing * jnp.einsum("hkt,hks->hts", query_full, key_full, precision=exact)
    score_grad = mixing * jnp.einsum("hvt,hvs->hts", out_grad, value_full, precision=exact)
    query_grad = jnp.einsum("hks,hts->hkt", key_full, score_grad, precision=exact)
    key_grad = jnp.einsum("hkt,hts->hks", query_full, score_grad, precision=exact)
    value_grad = jnp.einsum("hvt,hts->hvs", out_grad, scores, precision=exact)
    reach = score_scale * jnp.stack([from_start, toward_end])
    out_reach = out_grad[None] * reach[:, :, None, :]
    value_reach = value_full[None] * reach[:, :, None, :]
    key_reach = key_full[None] * reach[:, :, None, :]
    query_grad = query_grad + jnp.einsum("whvl,whkv->hkl", out_reach, key_carried, precision=exact)
    key_grad = key_grad + jnp.einsum("whvl,whkv->hkl", value_reach, query_carried, precision=exact)
    value_grad = value_grad + jnp.einsum("whkl,whkv->hvl", key_reach, query_carried, precision=exact)
    return (
        grad_gate,
        grad_up,
        grad_down,
        grad_proj,
        query_grad.reshape(heads_here * key_size, length),
        key_grad.reshape(heads_here * key_size, length),
        value_grad.reshape(heads_here * value_size, length),
    )


def solution(mesh):
    return jax.shard_map(
        on_device,
        mesh=mesh,
        in_specs=(
            P("sp", None),
            P("sp", None),
            P("sp", None),
            P("sp"),
            P("sp", None),
            P("sp", "tp"),
            P("tp", "sp"),
            P("tp", "sp"),
            P("tp", "sp"),
            P("tp", "sp"),
            P(None, "tp"),
            P("sp", None, "tp"),
            P("sp", None, "tp"),
            P("sp", "tp", None),
        ),
        out_specs=(
            P("sp", None, "tp"),
            P("sp", None, "tp"),
            P("sp", "tp", None),
            P("sp", "tp"),
            P("tp", "sp"),
            P("tp", "sp"),
            P("tp", "sp"),
        ),
        check_vma=False,
    )
```

time: 274 us -> 145 us (0.53)
  waiting for transfers between devices: 99.6 us -> 0 us
  Pallas kernels: 0 us -> 91.7 us
  blocking collectives: 66 us -> 0 us
  starting transfers between devices: 15.7 us -> 0 us
  local copies, waits for them, and re-layouts: 22.9 us -> 8.26 us
  between operations: 15.1 us -> 0.98 us
  other arithmetic: 16.2 us -> 9.84 us
  matrix products: 37 us -> 33.5 us
    pallas_call x0 -> x3, Pallas kernels: none -> 91.7 us  [the longest x1 39.1 us: dispatch(): pl.pallas_call(functools.partial(dispatch_kernel, sp_count, tp_count), ou...]
    all_to_all x3 -> x0, waiting for transfers between devices: 63.3 us -> none  [the longest x1 30.6 us: on_device(): lax.all_to_all(cot_rows, 'sp', split_axis=0, concat_axis=0, tiled=True)]
    all_gather x3 -> x0, blocking collectives: 50.9 us -> none  [the longest x2 40.5 us: carried_in(): gathered = jax.tree.map(lambda a: lax.all_gather(a, axis), part)]
    reduce_scatter x2 -> x0, waiting for transfers between devices: 36.2 us -> none  [the longest x1 19.2 us: on_device(): lax.psum_scatter(lax.dot_general(resid_grad, mixer_out, (((0,), (0,)), ((...]
    all_to_all x3 -> x0, starting transfers between devices: 15.4 us -> none  [the longest x1 6.49 us: on_device(): lax.all_to_all(inp_rows, 'sp', split_axis=0, concat_axis=0, tiled=True)]
    unnamed x1 -> x0, blocking collectives: 15.1 us -> none
    gather x5 -> x0, local copies, waits for them, and re-layouts: 13.3 us -> none  [the longest x1 6.16 us: pack_rows(): moe_input[token_ids]]
    add x8 -> x2, other arithmetic: 4.6 us -> 0.79 us  [the longest x1 0.78 us: slot_numbers(): slots.append(ids[:, j] * capacity + rank)]
  transfers between devices with their start and end apart: 5 -> 0, of which waited for: 5 -> 0; matrix products, arithmetic and copies ran while one was open for 17% -> 0% of each run, Pallas kernels for 0% -> 0%
where the time goes in v1:
time: 145 us; the launch traced here: 144 us
  Pallas kernels  91.7 us (63%)
  matrix products  33.5 us (23%)
  other arithmetic  9.84 us (7%)
  local copies, waits for them, and re-layouts  8.26 us (6%)
    pallas_call x1, Pallas kernels, dispatch(): pl.pallas_call(functools.partial(dispatch_kernel, sp_count, tp_count), ou...  39.1 us
    pallas_call x1, Pallas kernels, bring_back(): pl.pallas_call(functools.partial(return_kernel, sp_count, tp_count), out_...  31.8 us
    pallas_call x1, Pallas kernels, share(): pl.pallas_call(functools.partial(share_kernel, sp_count, tp_count), out_s...  20.8 us
    dot_general x1, matrix products, on_device(): jnp.einsum('secf,secd->efd', hidden, cot_blocks, preferred_element_type=j...  4.66 us
    dot_general x1, matrix products, expert_forward(): jnp.einsum('secd,edf->secf', inp_blocks, up_weight, preferred_element_typ...  3.15 us

profile of v1, /device:TPU:0, one launch (start us, length us, event | category | flops | bytes accessed | tf_op | source)
XLA Modules:
  0.0 144.3 jit_solution(16371100121469478044)
XLA Ops:
  4.9 1.0 fusion.21
  5.9 1.9 %convolution_convert_fusion.1 = bf16[384,512]{1,0:T(8,128)(2,1)} fusion(bf16[128,2048]{1,0:T(8,128)(2,1)} %param.15, s32[]{:T(128)S(6)} %select_n.59, s32[128]{0:T(128)S(1)} %get-tuple-element.25, s32[128]{0:T(128)S(1)} %get-tuple-element.26), kind=kOutput, calls=%fused_computation.22 | convolution fusion | flops 50675712 | bytes 525316 | tf_op jit(solution)/shard_map/dot_general | solution.py:415
  9.2 1.2 fusion.61
  11.1 1.0 convolution_bitcast_fusion.2
  12.1 1.3 concatenate.9.state
  13.4 39.1 %shard_map.189 = (bf16[8,48,2048]{2,1,0:T(8,128)(2,1)}, bf16[8,48,2048]{2,1,0:T(8,128)(2,1)}, f32[8,1,72,128]{3,2,1,0:T(8,128)}) custom-call(bf16[8,48,512]{2,1,0:T(8,128)(2,1)} %bitcast.183, bf16[8,48,512]{2,1,0:T(8,128)(2,1)} %bitcast.182, f32[2,1,72,128]{3,2,1,0:T(8,128)} %concatenate.9.state), custom_call_target="tpu_custom_call" | custom-call | tf_op jit(solution)/shard_map/pallas_call | solution.py:167
  52.5 3.1 %fusion.15 = f32[8,1,48,512]{3,2,0,1:T(8,128)S(1)} fusion(bf16[8,48,2048]{2,1,0:T(8,128)(2,1)} %get-tuple-element.12, bf16[1,2048,512]{2,1,0:T(8,128)(2,1)} %param.26), kind=kOutput, calls=%fused_computation.18 | convolution fusion | flops 805306368 | bytes 4456448 | tf_op jit(solution)/shard_map/secd,edf->secf/dot_general | solution.py:355
  55.7 1.0 fusion.18
  58.3 1.2 multiply_convert_fusion.1
  59.5 1.0 fusion.3
  61.1 2.2 %add_convert_fusion.part = bf16[8,48,2048]{2,1,0:T(8,128)(2,1)} fusion(f32[8,48,2048]{2,1,0:T(8,128)S(1)} %fusion.3, bf16[1,2048,512]{2,1,0:T(8,128)(2,1)S(1)} %copy-done.1, bf16[8,1,48,512]{3,2,0,1:T(8,128)(2,1)S(1)} %get-tuple-element.23), kind=kOutput, calls=%fused_computation.3 | convolution fusion | flops 806879232 | bytes 7208960 | tf_op jit(solution)/shard_map/secf,edf->secd/dot_general | solution.py:368
  64.2 31.8 %shard_map.190 = bf16[128,2048]{1,0:T(8,128)(2,1)} custom-call(bf16[8,48,2048]{2,1,0:T(8,128)(2,1)} %add_convert_fusion.part, bf16[8,128,48]{2,1,0:T(8,128)(2,1)} %or_convert_fusion.select, bf16[128,512]{1,0:T(8,128)(2,1)} %copy-done.2), custom_call_target="tpu_custom_call" | custom-call | tf_op jit(solution)/shard_map/pallas_call | solution.py:262
  96.0 2.2 %convolution_convert_fusion = bf16[2048,128]{1,0:T(8,128)(2,1)} fusion(bf16[128,2048]{1,0:T(8,128)(2,1)} %shard_map.190, bf16[128,128]{1,0:T(8,128)(2,1)S(1)} %copy-done.8), kind=kOutput, calls=%fused_computation.7 | convolution fusion | flops 67371008 | bytes 1081344 | tf_op jit(solution)/shard_map/dot_general | solution.py:474
  98.2 1.3 fusion.66
  100.4 20.8 %shard_map.191 = (f32[8,1,64,128]{3,2,1,0:T(8,128)}, bf16[8,256,128]{2,1,0:T(8,128)(2,1)}) custom-call(f32[2,1,64,128]{3,2,1,0:T(8,128)} %convolution_bitcast_fusion.1.state, bf16[8,256,128]{2,1,0:T(8,128)(2,1)} %bitcast.180), custom_call_target="tpu_custom_call" | custom-call | tf_op jit(solution)/shard_map/pallas_call | solution.py:320
  121.3 1.5 %slice_reduce_fusion = f32[8]{0:T(128)} fusion(f32[8,1,72,128]{3,2,1,0:T(8,128)} %get-tuple-element.15), kind=kLoop, calls=%fused_computation.86 | loop fusion | bytes 64 | tf_op jit(solution)/shard_map/slice | solution.py:488
  123.6 1.0 slice_bitcast_fusion
  124.6 1.7 %multiply_reduce_fusion = (f32[2,64,128]{2,1,0:T(8,128)S(1)}, f32[2,64,128]{2,1,0:T(8,128)}) fusion(f32[8,64,128]{2,1,0:T(8,128)} %bitcast.184, f32[2,8]{1,0:T(2,128)S(1)} %bitcast.189, f32[8,64,128]{2,1,0:T(8,128)S(1)} %slice_bitcast_fusion), kind=kLoop, calls=%fused_computation.40 | loop fusion | flops 491520 | bytes 655424 | tf_op jit(solution)/shard_map/reduce_sum | solution.py:498
  127.2 0.9 convolution_multiply_fusion.1
  129.1 0.9 convolution_multiply_fusion.2
  132.0 1.7 %fusion.23 = f32[64,128]{1,0:T(8,128)} fusion(f32[64,128]{1,0:T(8,128)S(1)} %convolution_bitcast_fusion.6, f32[2,64,128]{2,1,0:T(8,128)} %get-tuple-element.20, f32[2,128]{1,0:T(2,128)} %copy-done.9, f32[128,128]{1,0:T(8,128)} %copy.24), kind=kOutput, calls=%fused_computation.33 | convolution fusion | flops 25206784 | bytes 197632 | tf_op jit(solution)/shard_map/whvl,whkv->hkl/dot_general | solution.py:509
  134.4 4.7 %fusion.2 = bf16[1,512,2048]{2,1,0:T(8,128)(2,1)} fusion(bf16[8,48,2048]{2,1,0:T(8,128)(2,1)} %get-tuple-element.13, f32[8,1,48,512]{3,2,0,1:T(8,128)} %copy-done.17, f32[8,1,48,512]{3,2,0,1:T(8,128)} %copy-done.18), kind=kOutput, calls=%fused_computation.6 | convolution fusion | flops 807534592 | bytes 5242880 | tf_op jit(solution)/shard_map/secf,secd->efd/dot_general | solution.py:464
  139.1 2.6 %fusion.1 = bf16[1,2048,512]{2,1,0:T(8,128)(2,1)} fusion(bf16[8,48,2048]{2,1,0:T(8,128)(2,1)S(1)} %copy-done.15, bf16[8,1,48,512]{3,2,0,1:T(8,128)(2,1)S(1)} %get-tuple-element.23), kind=kOutput, calls=%fused_computation.5 | convolution fusion | flops 806354944 | bytes 4063232 | tf_op jit(solution)/shard_map/secd,secf->edf/dot_general | solution.py:470
  141.7 2.6 %fusion = bf16[1,2048,512]{2,1,0:T(8,128)(2,1)} fusion(bf16[8,48,2048]{2,1,0:T(8,128)(2,1)S(1)} %copy-done.15, bf16[8,1,48,512]{3,2,0,1:T(8,128)(2,1)S(1)} %get-tuple-element.24), kind=kOutput, calls=%fused_computation.4 | convolution fusion | flops 806354944 | bytes 4063232 | tf_op jit(solution)/shard_map/secd,secf->edf/dot_general | solution.py:467
  (69 shorter events, 15.6 us)
Async XLA Ops:
  0.6 55.0 %copy-start = (bf16[1,2048,512]{2,1,0:T(8,128)(2,1)S(1)}, bf16[1,2048,512]{2,1,0:T(8,128)(2,1)}, u32[]{:S(2)}) copy-start(bf16[1,2048,512]{2,1,0:T(8,128)(2,1)} %param.25) | copy-start | bytes 6291460
  4.9 50.7 %copy-start.2 = (bf16[128,512]{1,0:T(8,128)(2,1)}, bf16[128,512]{1,0:T(8,128)(2,1)S(1)}, u32[]{:S(2)}) copy-start(bf16[128,512]{1,0:T(8,128)(2,1)S(1)} %constant_dynamic-slice_fusion.cot) | copy-start | bytes 393220
  8.6 1.8 %copy-start.12 = (f32[1,128]{1,0:T(1,128)}, f32[1,128]{1,0:T(1,128)S(1)}, u32[]{:S(2)}) copy-start(f32[1,128]{1,0:T(1,128)S(1)} %fusion.48) | copy-start | bytes 1540
  10.4 45.2 %copy-start.10 = (f32[2,1,128]{2,1,0:T(1,128)}, f32[2,1,128]{2,1,0:T(1,128)S(1)}, u32[]{:S(2)}) copy-start(f32[2,1,128]{2,1,0:T(1,128)S(1)} %pad_maximum_fusion) | copy-start | bytes 3076
  52.5 3.2 %copy-start.14 = (bf16[8,48,2048]{2,1,0:T(8,128)(2,1)S(1)}, bf16[8,48,2048]{2,1,0:T(8,128)(2,1)}, u32[]{:S(2)}) copy-start(bf16[8,48,2048]{2,1,0:T(8,128)(2,1)} %get-tuple-element.12) | copy-start | bytes 4718596
  55.7 1.0 copy-start.17
  55.7 1.9 %copy-start.13 = (bf16[1,512,2048]{2,1,0:T(8,128)(2,1)S(1)}, bf16[1,512,2048]{2,1,0:T(8,128)(2,1)}, u32[]{:S(2)}) copy-start(bf16[1,512,2048]{2,1,0:T(8,128)(2,1)} %param.27) | copy-start | bytes 6291460
  55.7 2.6 %copy-start.16 = (bf16[8,48,2048]{2,1,0:T(8,128)(2,1)S(1)}, bf16[8,48,2048]{2,1,0:T(8,128)(2,1)}, u32[]{:S(2)}) copy-start(bf16[8,48,2048]{2,1,0:T(8,128)(2,1)} %get-tuple-element.13) | copy-start | bytes 4718596
  56.7 2.8 %copy-start.18 = (f32[8,1,48,512]{3,2,0,1:T(8,128)}, f32[8,1,48,512]{3,2,0,1:T(8,128)S(1)}, u32[]{:S(2)}) copy-start(f32[8,1,48,512]{3,2,0,1:T(8,128)S(1)} %fusion.18) | copy-start | bytes 2359300
  59.5 1.6 %copy-start.1 = (bf16[1,2048,512]{2,1,0:T(8,128)(2,1)S(1)}, bf16[1,2048,512]{2,1,0:T(8,128)(2,1)}, u32[]{:S(2)}) copy-start(bf16[1,2048,512]{2,1,0:T(8,128)(2,1)} %param.26) | copy-start | bytes 6291460
  63.3 32.7 %copy-start.8 = (bf16[128,128]{1,0:T(8,128)(2,1)S(1)}, bf16[128,128]{1,0:T(8,128)(2,1)}, u32[]{:S(2)}) copy-start(bf16[128,128]{1,0:T(8,128)(2,1)} %param.19) | copy-start | bytes 98308
  63.3 34.9 %copy-start.4 = (bf16[2048,128]{1,0:T(8,128)(2,1)S(1)}, bf16[2048,128]{1,0:T(8,128)(2,1)}, u32[]{:S(2)}) copy-start(bf16[2048,128]{1,0:T(8,128)(2,1)} %param.24) | copy-start | bytes 1572868
  64.2 35.4 %copy-start.6 = (bf16[64,128]{1,0:T(8,128)(2,1)S(1)}, bf16[64,128]{1,0:T(8,128)(2,1)}, u32[]{:S(2)}) copy-start(bf16[64,128]{1,0:T(8,128)(2,1)} %param.20) | copy-start | bytes 49156
  96.0 3.6 %copy-start.11 = (f32[2,1,128]{2,1,0:T(1,128)S(1)}, f32[2,1,128]{2,1,0:T(1,128)}, u32[]{:S(2)}) copy-start(f32[2,1,128]{2,1,0:T(1,128)} %copy-done.10) | copy-start | bytes 3076
  98.2 30.9 %copy-start.5 = (bf16[128,128]{1,0:T(8,128)(2,1)S(1)}, bf16[128,128]{1,0:T(8,128)(2,1)}, u32[]{:S(2)}) copy-start(bf16[128,128]{1,0:T(8,128)(2,1)} %param.22) | copy-start | bytes 98308
  121.3 12.4 %copy-start.3 = (bf16[8,256,128]{2,1,0:T(8,128)(2,1)S(1)}, bf16[8,256,128]{2,1,0:T(8,128)(2,1)}, u32[]{:S(2)}) copy-start(bf16[8,256,128]{2,1,0:T(8,128)(2,1)} %get-tuple-element.14) | copy-start | bytes 1572868
  122.8 8.3 %copy-start.7 = (bf16[64,128]{1,0:T(8,128)(2,1)S(1)}, bf16[64,128]{1,0:T(8,128)(2,1)}, u32[]{:S(2)}) copy-start(bf16[64,128]{1,0:T(8,128)(2,1)} %param.21) | copy-start | bytes 49156
  126.9 4.3 %copy-start.9 = (f32[2,128]{1,0:T(2,128)}, f32[2,128]{1,0:T(2,128)S(1)}, u32[]{:S(2)}) copy-start(f32[2,128]{1,0:T(2,128)S(1)} %maximum_multiply_fusion) | copy-start | bytes 3076
  134.4 4.7 %copy-start.15 = (bf16[8,48,2048]{2,1,0:T(8,128)(2,1)S(1)}, bf16[8,48,2048]{2,1,0:T(8,128)(2,1)}, u32[]{:S(2)}) copy-start(bf16[8,48,2048]{2,1,0:T(8,128)(2,1)} %get-tuple-element.12) | copy-start | bytes 4718596

commit v2 on v1

--- a/solution.py
+++ b/solution.py
@@ -20,7 +20,7 @@
     return order
 
 
-def greet(sp_count, tp_count, sp_place, tp_place, along_tp):
+def greet_all(sp_count, tp_count, sp_place, tp_place, along_tp):
     barrier = pltpu.get_barrier_semaphore()
     for k in range(1, sp_count):
         pl.semaphore_signal(
@@ -37,7 +37,16 @@
                 device_id={"sp": sp_place, "tp": lax.rem(tp_place + m, tp_count)},
                 device_id_type=MESH,
             )
+
+
+def greet_wait(sp_count, tp_count, along_tp):
+    barrier = pltpu.get_barrier_semaphore()
     pl.semaphore_wait(barrier, sp_count - 1 + (tp_count - 1 if along_tp else 0))
+
+
+def greet(sp_count, tp_count, sp_place, tp_place, along_tp):
+    greet_all(sp_count, tp_count, sp_place, tp_place, along_tp)
+    greet_wait(sp_count, tp_count, along_tp)
 
 
 def remote(src, dst, send_sem, recv_sem, sp_place, tp_place):
@@ -56,8 +65,8 @@
 
 
 def dispatch_kernel(
-    sp_count, tp_count, cot_src, inp_src, state, cot_full, inp_full, state_all,
-    local_sem, send_one, recv_one, send_two, recv_two, send_state, recv_state,
+    sp_count, tp_count, capacity, ids, group, weight, cot, inp, keys, values, rates,
+    cot_full, inp_full, state_all, select, cot_src, inp_src, state, local_sem, send_one, recv_one, send_two, recv_two, send_state, recv_state,
 ):
     me = lax.axis_index("sp")
     q = lax.axis_index("tp")
@@ -79,23 +88,97 @@
         peers = tuple(lax.rem(q + m, tp_count) for m in range(1, tp_count))
         origins = tuple(lax.rem(q + tp_count - m, tp_count) for m in range(1, tp_count))
 
-    greet(sp_count, tp_count, me, q, True)
+    greet_all(sp_count, tp_count, me, q, True)
+    tokens, top_count = ids.shape
+    block_rows = cot_src.shape[1]
+    experts_all = sp_count * block_rows // capacity
+    mine = pl.ds(pl.multiple_of(q * width, width), width)
+    expert = lax.broadcasted_iota(jnp.int32, (tokens, experts_all), 1)
+    named = [(ids[:, j : j + 1] == expert).astype(jnp.float32) for j in range(top_count)]
+    below = lax.broadcasted_iota(jnp.int32, (tokens, tokens), 0) > lax.broadcasted_iota(
+        jnp.int32, (tokens, tokens), 1
+    )
+    before = jnp.dot(
+        below.astype(jnp.float32).astype(jnp.bfloat16),
+        sum(named).astype(jnp.bfloat16),
+        preferred_element_type=jnp.float32,
+    )
+    slots = []
+    scaled = []
+    cot_mine = cot[:, mine].astype(jnp.float32)
+    inp_mine = inp[:, mine]
+    for j in range(top_count):
+        rank = jnp.sum(named[j] * before, axis=1, keepdims=True).astype(jnp.int32)
+        before = before + named[j]
+        slots.append(ids[:, j : j + 1] * capacity + rank)
+        scaled.append((cot_mine * (group[...] * weight[:, j : j + 1])).astype(jnp.bfloat16))
+    slot = lax.broadcasted_iota(jnp.int32, (tokens, block_rows), 1)
+
+    def rows_of(picked, values):
+        return lax.dot_general(
+            picked, values, (((0,), (0,)), ((), ())), preferred_element_type=jnp.float32
+        )
+
+    def pack(k):
+        there = lax.rem(me + k, sp_count)
+        picks = [
+            (s == slot + there * block_rows).astype(jnp.float32).astype(jnp.bfloat16)
+            for s in slots
+        ]
+        cot_src[there] = sum(rows_of(p, v) for p, v in zip(picks, scaled)).astype(jnp.bfloat16)
+        either = sum(picks)
+        inp_src[there] = rows_of(either, inp_mine).astype(jnp.bfloat16)
+        select[there] = either
+        return there
+
     waits = []
     own = []
+    pack(0)
+    pack(order[1])
+    greet_wait(sp_count, tp_count, True)
     for a, (src, full) in enumerate(arrays):
         copy = pltpu.make_async_copy(src.at[me], columns(full, me, q), local_sem.at[a])
         copy.start()
         own.append(copy)
-    own_state = pltpu.make_async_copy(state.at[0], state_all.at[me], local_sem.at[2])
-    own_state.start()
     for k in order[1:]:
         there = lax.rem(me + k, sp_count)
+        if k != order[1]:
+            pack(k)
         for a, (src, full) in enumerate(arrays):
             copy = remote(
                 src.at[there], columns(full, me, q), send_one.at[a, k], recv_one.at[a, k], there, q
             )
             copy.start()
             waits.append(copy)
+    exact = lax.Precision.HIGHEST
+    heads, length = rates.shape
+    key_size = keys.shape[0] // heads
+    value_size = values.shape[0] // heads
+    upto = lax.broadcasted_iota(jnp.int32, (length, length), 0) <= lax.broadcasted_iota(
+        jnp.int32, (length, length), 1
+    )
+    for h in range(heads):
+        rate = jnp.broadcast_to(rates[h : h + 1, :], (8, length))
+        prefix = jnp.dot(
+            rate, upto.astype(jnp.float32), precision=exact, preferred_element_type=jnp.float32
+        )[0:1]
+        ending = prefix[:, length - 1 : length]
+        key = keys[h * key_size : (h + 1) * key_size, :].astype(jnp.float32)
+        value = values[h * value_size : (h + 1) * value_size, :].astype(jnp.float32)
+        first = h * (key_size + 8)
+        for side, reach in enumerate((jnp.exp(prefix - ending), jnp.exp(-prefix))):
+            state[side, first : first + key_size, :] = lax.dot_general(
+                key * reach,
+                value,
+                (((1,), (1,)), ((), ())),
+                precision=exact,
+                preferred_element_type=jnp.float32,
+            )
+            state[side, first + key_size : first + key_size + 8, :] = jnp.broadcast_to(
+                ending, (8, value_size)
+            )
+    own_state = pltpu.make_async_copy(state.at[0], state_all.at[me], local_sem.at[2])
+    own_state.start()
     for k in order[1:]:
         there = lax.rem(me + k, sp_count)
         copy = remote(
@@ -160,16 +243,28 @@
         copy.wait_send()
 
 
-def dispatch(cot_src, inp_src, state, sp_count, tp_count):
-    rows, width = cot_src.shape[1:]
-    full = jax.ShapeDtypeStruct((sp_count, rows, width * tp_count), cot_src.dtype)
+def dispatch(ids, group, weight, cot, inp, keys, values, rates, capacity, rows, sp_count, tp_count):
+    tokens, model_width = cot.shape
+    width = model_width // tp_count
+    heads = rates.shape[0]
+    state_rows = keys.shape[0] + 8 * heads
+    value_size = values.shape[0] // heads
+    full = jax.ShapeDtypeStruct((sp_count, rows, model_width), cot.dtype)
     dma = pltpu.SemaphoreType.DMA
     return pl.pallas_call(
-        functools.partial(dispatch_kernel, sp_count, tp_count),
-        out_shape=(full, full, jax.ShapeDtypeStruct((sp_count,) + state.shape[1:], state.dtype)),
-        in_specs=[VMEM] * 3,
-        out_specs=(VMEM,) * 3,
+        functools.partial(dispatch_kernel, sp_count, tp_count, capacity),
+        out_shape=(
+            full,
+            full,
+            jax.ShapeDtypeStruct((sp_count, state_rows, value_size), jnp.float32),
+            jax.ShapeDtypeStruct((sp_count, tokens, rows), jnp.bfloat16),
+        ),
+        in_specs=[VMEM] * 8,
+        out_specs=(VMEM,) * 4,
         scratch_shapes=[
+            pltpu.VMEM((sp_count, rows, width), cot.dtype),
+            pltpu.VMEM((sp_count, rows, width), inp.dtype),
+            pltpu.VMEM((2, state_rows, value_size), jnp.float32),
             dma((3,)),
             dma((2, sp_count)),
             dma((2, sp_count)),
@@ -179,7 +274,7 @@
             dma((sp_count,)),
         ],
         compiler_params=pltpu.CompilerParams(collective_id=0, has_side_effects=True),
-    )(cot_src, inp_src, state)
+    )(ids, group, weight, cot, inp, keys, values, rates)
 
 
 def return_kernel(
@@ -188,7 +283,7 @@
 ):
     me = lax.axis_index("sp")
     q = lax.axis_index("tp")
-    width = cot.shape[1]
+    width = cot.shape[1] // tp_count
     order = near_first(sp_count)
 
     def columns(place):
@@ -240,7 +335,7 @@
         total = total + jnp.dot(
             select[source], returned[source], preferred_element_type=jnp.float32
         )
-    resid[:, columns(q)] = (cot[...].astype(jnp.float32) + total).astype(resid.dtype)
+    resid[:, columns(q)] = (cot[:, columns(q)].astype(jnp.float32) + total).astype(resid.dtype)
     for m in range(1, tp_count):
         piece = resid.at[:, columns(q)]
         copy = remote(
@@ -255,13 +350,13 @@
         copy.wait_send()
 
 
-def bring_back(part, select, cot_slice, sp_count, tp_count):
+def bring_back(part, select, cot, sp_count, tp_count):
     rows = part.shape[1]
-    tokens, width = cot_slice.shape
+    width = cot.shape[1] // tp_count
     dma = pltpu.SemaphoreType.DMA
     return pl.pallas_call(
         functools.partial(return_kernel, sp_count, tp_count),
-        out_shape=jax.ShapeDtypeStruct((tokens, width * tp_count), cot_slice.dtype),
+        out_shape=jax.ShapeDtypeStruct(cot.shape, cot.dtype),
         in_specs=[VMEM] * 3,
         out_specs=VMEM,
         scratch_shapes=[
@@ -276,76 +371,7 @@
             dma((tp_count - 1,)),
         ],
         compiler_params=pltpu.CompilerParams(collective_id=1, has_side_effects=True),
-    )(part, select, cot_slice)
-
-
-def share_kernel(
-    sp_count, tp_count, state, proj, state_all, proj_all,
-    local_sem, send_state, recv_state, send_proj, recv_proj,
-):
-    me = lax.axis_index("sp")
-    q = lax.axis_index("tp")
-    order = near_first(sp_count)[1:][::-1]
-    greet(sp_count, tp_count, me, q, False)
-    own_state = pltpu.make_async_copy(state.at[0], state_all.at[me], local_sem.at[0])
-    own_proj = pltpu.make_async_copy(proj.at[me], proj_all.at[me], local_sem.at[1])
-    own_state.start()
-    own_proj.start()
-    waits = []
-    for k in order:
-        there = lax.rem(me + k, sp_count)
-        side = state_side(me, there, sp_count)
-        for copy in (
-            remote(state.at[side], state_all.at[me], send_state.at[k], recv_state.at[k], there, q),
-            remote(proj.at[there], proj_all.at[me], send_proj.at[k], recv_proj.at[k], there, q),
-        ):
-            copy.start()
-            waits.append(copy)
-    own_state.wait()
-    own_proj.wait()
-    for k in order:
-        source = lax.rem(me + sp_count - k, sp_count)
-        remote(
-            state.at[0], state_all.at[source], send_state.at[k], recv_state.at[k], me, q
-        ).wait_recv()
-        remote(
-            proj.at[source], proj_all.at[source], send_proj.at[k], recv_proj.at[k], me, q
-        ).wait_recv()
-    for copy in waits:
-        copy.wait_send()
-
-
-def share(state, proj, sp_count, tp_count):
-    dma = pltpu.SemaphoreType.DMA
-    return pl.pallas_call(
-        functools.partial(share_kernel, sp_count, tp_count),
-        out_shape=(
-            jax.ShapeDtypeStruct((sp_count,) + state.shape[1:], state.dtype),
-            jax.ShapeDtypeStruct(proj.shape, proj.dtype),
-        ),
-        in_specs=[VMEM] * 2,
-        out_specs=(VMEM,) * 2,
-        scratch_shapes=[
-            dma((2,)), dma((sp_count,)), dma((sp_count,)), dma((sp_count,)), dma((sp_count,)),
-        ],
-        compiler_params=pltpu.CompilerParams(collective_id=2, has_side_effects=True),
-    )(state, proj)
-
-
-def slot_numbers(ids, experts_all, capacity):
-    rows, top_count = ids.shape
-    onehot = ids[:, :, None] == jnp.arange(experts_all, dtype=jnp.int32)
-    row_tally = jnp.sum(onehot.astype(jnp.float32), axis=1)
-    place = jnp.arange(rows, dtype=jnp.int32)
-    below = (place[:, None] > place[None, :]).astype(jnp.bfloat16)
-    before = jnp.dot(below, row_tally.astype(jnp.bfloat16), preferred_element_type=jnp.float32)
-    slots = []
-    for j in range(top_count):
-        here = onehot[:, j].astype(jnp.float32)
-        rank = jnp.sum(here * before, axis=1).astype(jnp.int32)
-        before = before + here
-        slots.append(ids[:, j] * capacity + rank)
-    return slots
+    )(part, select, cot)
 
 
 def expert_forward(cot_blocks, inp_blocks, gate_weight, up_weight, down_weight):
@@ -396,23 +422,6 @@
     rows_here, model_width = cotangent.shape
     top_count = expert_ids.shape[1]
     capacity = 3 * top_count * rows_here // (2 * experts_all)
-    slice_width = model_width // tp_count
-    offset = lax.axis_index("tp") * slice_width
-    slot_count = experts_all * capacity
-
-    slots = slot_numbers(expert_ids, experts_all, capacity)
-    slot_range = jnp.arange(slot_count, dtype=jnp.int32)
-    hits = [slot_range[:, None] == s[None, :] for s in slots]
-    select = functools.reduce(jnp.logical_or, hits).astype(jnp.bfloat16)
-    route = group_weight[:, None] * expert_weight
-    row_scale = sum(
-        jnp.sum(jnp.where(h, route[:, j][None, :], 0.0), axis=1) for j, h in enumerate(hits)
-    )
-    cot_slice = lax.dynamic_slice_in_dim(cotangent, offset, slice_width, 1)
-    inp_slice = lax.dynamic_slice_in_dim(moe_input, offset, slice_width, 1)
-    cot_rows = jnp.dot(select, cot_slice, preferred_element_type=jnp.float32)
-    cot_rows = (cot_rows * row_scale[:, None]).astype(jnp.bfloat16)
-    inp_rows = jnp.dot(select, inp_slice, preferred_element_type=jnp.float32).astype(jnp.bfloat16)
     block_rows = local_experts * capacity
 
     heads_here, length = decay_rates.shape
@@ -431,21 +440,21 @@
     toward_end = jnp.exp(prefix - ending)
     from_start = jnp.exp(-prefix)
     both_weights = jnp.stack([toward_end, from_start])
-    key_state = jnp.einsum(
-        "whkl,hvl->whkv", key_full[None] * both_weights[:, :, None, :], value_full, precision=exact
-    )
-    totals_rows = jnp.broadcast_to(
-        ending[None, :, :, None], (2, heads_here, 8, value_size)
-    )
-    key_state = jnp.concatenate([key_state, totals_rows], axis=2)
-
-    got_cot, got_inp, key_states = dispatch(
-        cot_rows.reshape(sp_count, block_rows, slice_width),
-        inp_rows.reshape(sp_count, block_rows, slice_width),
-        key_state,
+    got_cot, got_inp, key_states, select = dispatch(
+        expert_ids,
+        group_weight[:, None],
+        expert_weight,
+        cotangent,
+        moe_input,
+        key_vectors,
+        value_vectors,
+        decay_rates,
+        capacity,
+        block_rows,
         sp_count,
         tp_count,
     )
+    key_states = key_states.reshape(sp_count, heads_here, -1, value_size)
     block_shape = (sp_count, local_experts, capacity, model_width)
     cot_blocks = got_cot.reshape(block_shape)
     inp_blocks = got_inp.reshape(block_shape)
@@ -453,13 +462,8 @@
         cot_blocks, inp_blocks, gate_weight, up_weight, down_weight
     )
 
-    select_back = select.reshape(sp_count, block_rows, rows_here).transpose(0, 2, 1)
     resid_grad = bring_back(
-        partial_grad.reshape(sp_count, block_rows, model_width),
-        select_back,
-        cot_slice,
-        sp_count,
-        tp_count,
+        partial_grad.reshape(sp_count, block_rows, model_width), select, cotangent, sp_count, tp_count
     )
     grad_down = jnp.einsum(
         "secf,secd->efd", hidden, cot_blocks, preferred_element_type=jnp.float32
@@ -480,13 +484,24 @@
     query_state = jnp.einsum(
         "whkl,hvl->whkv", query_full[None] * both_weights[:, :, None, :], out_grad, precision=exact
     )
-    query_states, proj_parts = share(
-        query_state, proj_part.reshape(sp_count, model_width // sp_count, -1), sp_count, tp_count
-    )
-    grad_proj = jnp.sum(proj_parts.astype(jnp.float32), axis=0)
+    block = jnp.arange(sp_count, dtype=jnp.int32)
+    query_state = query_state.astype(jnp.bfloat16).transpose(0, 2, 1, 3)
+    query_state = query_state.reshape(2, key_size, heads_here * value_size)
+    sent = jnp.concatenate(
+        [
+            proj_part.reshape(sp_count, -1, heads_here * value_size),
+            jnp.where((block > me)[:, None, None], query_state[:1], query_state[1:]),
+        ],
+        axis=1,
+    )
+    shared = lax.all_to_all(sent, "sp", split_axis=0, concat_axis=0, tiled=True)
+    shared = shared.astype(jnp.float32)
+    proj_rows = model_width // sp_count
+    grad_proj = jnp.sum(shared[:, :proj_rows], axis=0)
+    query_states = shared[:, proj_rows:].reshape(sp_count, key_size, heads_here, value_size)
+    query_states = query_states.transpose(0, 2, 1, 3)
 
     totals = key_states[:, :, key_size, 0]
-    block = jnp.arange(sp_count, dtype=jnp.int32)
     low_between = (block[None, :] > block[:, None]) & (block[None, :] < me)
     high_between = (block[None, :] < block[:, None]) & (block[None, :] > me)
     low_decay = jnp.exp(-jnp.sum(jnp.where(low_between[:, :, None], totals[None], 0.0), axis=1))

time: 145 us -> 122 us (0.84)
  Pallas kernels: 91.7 us -> 71.7 us
  other arithmetic: 9.84 us -> 5.75 us
  starting transfers between devices: 0 us -> 3.78 us
  matrix products: 33.5 us -> 30.2 us
    pallas_call x2 -> x1, Pallas kernels: 59.9 us -> 40.6 us  [dispatch(): pl.pallas_call(functools.partial(dispatch_kernel, sp_count, tp_count, cap...]
    dot_general x4 -> x0, matrix products: 4.03 us -> none  [the longest x1 1.91 us: on_device(): jnp.dot(select, inp_slice, preferred_element_type=jnp.float32)]
    all_to_all x0 -> x1, starting transfers between devices: none -> 3.78 us  [on_device(): shared = lax.all_to_all(sent, 'sp', split_axis=0, concat_axis=0, tiled=True)]
    unnamed x38 -> x48, local copies, waits for them, and re-layouts: 2.26 us -> 4.69 us
    dot_general x1, matrix products: 4.66 us -> 2.67 us  [on_device(): jnp.einsum('secf,secd->efd', hidden, cot_blocks, preferred_element_type=j...]
    dot_general x1, matrix products: 2.61 us -> 4.24 us  [on_device(): jnp.einsum('secd,secf->edf', inp_blocks, gate_grad, preferred_element_typ...]
    reduce_sum x1, other arithmetic: 1.75 us -> 0.14 us  [on_device(): query_carried = jnp.sum(both_decays * query_states[None], axis=1)]
  transfers between devices with their start and end apart: 0 -> 1, of which waited for: 0 -> 0; matrix products, arithmetic and copies ran while one was open for 0% -> 17% of each run, Pallas kernels for 0% -> 0%
where the time goes in v2:
time: 122 us
  Pallas kernels  71.7 us (59%)
  matrix products  30.2 us (25%)
  local copies, waits for them, and re-layouts  9.15 us (8%)
  other arithmetic  5.75 us (5%)
  starting transfers between devices  3.78 us (3%)
    pallas_call x1, Pallas kernels, dispatch(): pl.pallas_call(functools.partial(dispatch_kernel, sp_count, tp_count, cap...  40.6 us
    pallas_call x1, Pallas kernels, bring_back(): pl.pallas_call(functools.partial(return_kernel, sp_count, tp_count), out_...  31.1 us
    unnamed x48, local copies, waits for them, and re-layouts  4.69 us
    dot_general x1, matrix products, on_device(): jnp.einsum('secd,secf->edf', inp_blocks, gate_grad, preferred_element_typ...  4.24 us
    dot_general x1, matrix products, on_device(): jnp.einsum('secd,secf->edf', inp_blocks, up_grad, preferred_element_type=...  4.02 us
    all_to_all x1, starting transfers between devices, on_device(): shared = lax.all_to_all(sent, 'sp', split_axis=0, concat_axis=0, tiled=True)  3.78 us
    dot_general x1, matrix products, expert_forward(): jnp.einsum('secd,edf->secf', inp_blocks, up_weight, preferred_element_typ...  3.15 us
    dot_general x1, matrix products, on_device(): jnp.einsum('secf,secd->efd', hidden, cot_blocks, preferred_element_type=j...  2.67 us
  transfers between devices with their start and end apart: 1, of which 0 were waited for; matrix products, arithmetic and copies ran while one was open for 17% of the time, Pallas kernels for 0%

profile of v2, /device:TPU:0, one launch (start us, length us, event | category | flops | bytes accessed | tf_op | source)
XLA Modules:
  0.0 121.7 jit_solution(2256011318502300169)
XLA Ops:
  0.7 1.6 %copy.29.ids = s32[128,2]{1,0:T(8,128)} copy(s32[128,2]{0,1:T(2,128)} %param.16) | data formatting | bytes 2048 | tf_op args[2]
  2.2 1.4 %copy.30.group = f32[128,1]{1,0:T(8,128)} copy(f32[128,1]{0,1:T(1,128)} %bitcast.162) | data formatting | bytes 1024 | tf_op jit(solution)/shard_map/broadcast_in_dim | solution.py:445
  3.6 1.4 %copy.31.weight = f32[128,2]{1,0:T(8,128)} copy(f32[128,2]{0,1:T(2,128)} %param.18) | data formatting | bytes 2048 | tf_op args[4]
  5.8 40.6 %shard_map.189 = (bf16[8,48,2048]{2,1,0:T(8,128)(2,1)}, bf16[8,48,2048]{2,1,0:T(8,128)(2,1)}, f32[8,72,128]{2,1,0:T(8,128)}, bf16[8,128,48]{2,1,0:T(8,128)(2,1)}) custom-call(s32[128,2]{1,0:T(8,128)} %copy.29.ids, f32[128,1]{1,0:T(8,128)} %copy.30.group, f32[128,2]{1,0:T(8,128)} %copy.31.weight, bf16[128,2048]{1,0:T(8,128)(2,1)} %cot.3, ...), custom_call_target="tpu_custom_call" | custom-call | tf_op jit(solution)/shard_map/pallas_call | solution.py:254
  46.5 3.1 %fusion.15 = f32[8,1,48,512]{3,2,0,1:T(8,128)S(1)} fusion(bf16[8,48,2048]{2,1,0:T(8,128)(2,1)} %get-tuple-element.11, bf16[1,2048,512]{2,1,0:T(8,128)(2,1)} %param.26), kind=kOutput, calls=%fused_computation.18 | convolution fusion | flops 805306368 | bytes 4456448 | tf_op jit(solution)/shard_map/secd,edf->secf/dot_general | solution.py:381
  49.7 1.0 fusion.18
  52.3 1.2 %multiply_convert_fusion.1 = (bf16[8,1,48,512]{3,2,0,1:T(8,128)(2,1)S(1)}, bf16[8,1,48,512]{3,2,0,1:T(8,128)(2,1)S(1)}) fusion(f32[8,1,48,512]{3,2,0,1:T(8,128)S(1)} %fusion.18, f32[8,1,48,512]{3,2,0,1:T(8,128)S(1)} %fusion.15, bf16[8,48,2048]{2,1,0:T(8,128)(2,1)S(1)} %copy-done.16, bf16[1,512,2048]{2,1,0:T(8,128)(2,1)S(1)} %copy-done.15), kind=kOutput, calls=%fused_computation.34 | convolution fusion | flops 807862272 | bytes 6029312 | tf_op jit(solution)/shard_map/secd,efd->secf/dot_general | solution.py:384
  53.5 1.0 fusion.3
  55.1 1.2 fusion.46
  56.3 2.2 %add_convert_fusion.part = bf16[8,48,2048]{2,1,0:T(8,128)(2,1)} fusion(f32[8,48,2048]{2,1,0:T(8,128)S(1)} %fusion.3, bf16[1,2048,512]{2,1,0:T(8,128)(2,1)S(1)} %copy-done.1, bf16[8,1,48,512]{3,2,0,1:T(8,128)(2,1)S(1)} %get-tuple-element.19), kind=kOutput, calls=%fused_computation.3 | convolution fusion | flops 806879232 | bytes 7208960 | tf_op jit(solution)/shard_map/secf,edf->secd/dot_general | solution.py:394
  58.5 31.1 %shard_map.190 = bf16[128,2048]{1,0:T(8,128)(2,1)} custom-call(bf16[8,48,2048]{2,1,0:T(8,128)(2,1)} %add_convert_fusion.part, bf16[8,128,48]{2,1,0:T(8,128)(2,1)} %get-tuple-element.13.select, bf16[128,2048]{1,0:T(8,128)(2,1)} %cot.3), custom_call_target="tpu_custom_call" | custom-call | tf_op jit(solution)/shard_map/pallas_call | solution.py:357
  89.7 1.3 %fusion.51 = f32[128,128]{1,0:T(8,128)S(1)} fusion(bf16[128,2048]{1,0:T(8,128)(2,1)} %shard_map.190, bf16[2048,128]{1,0:T(8,128)(2,1)S(1)} %copy-done.2), kind=kOutput, calls=%fused_computation.87 | convolution fusion | flops 67108864 | bytes 1114112 | tf_op jit(solution)/shard_map/dot_general | solution.py:481
  91.3 1.4 %convolution_convert_fusion = bf16[2048,128]{1,0:T(8,128)(2,1)S(1)} fusion(bf16[128,2048]{1,0:T(8,128)(2,1)} %shard_map.190, bf16[128,128]{1,0:T(8,128)(2,1)S(1)} %copy-done.10), kind=kOutput, calls=%fused_computation.7 | convolution fusion | flops 67371008 | bytes 1081344 | tf_op jit(solution)/shard_map/dot_general | solution.py:478
  92.8 0.9 pad_maximum_fusion
  93.7 3.8 %all-to-all-start = ((bf16[8,320,128]{2,1,0:T(8,128)(2,1)}), bf16[8,320,128]{2,1,0:T(8,128)(2,1)S(1)}, u32[]{:S(2)}, u32[]{:S(2)}) async-start(bf16[8,320,128]{2,1,0:T(8,128)(2,1)} %pad_maximum_fusion), calls=%async_computation | async-start | bytes 1310720 | tf_op jit(solution)/shard_map/all_to_all | solution.py:497
  98.0 1.4 %slice_reduce_fusion.1 = f32[8]{0:T(128)} fusion(f32[8,1,72,128]{3,2,0,1:T(8,128)} %bitcast.156), kind=kLoop, calls=%fused_computation.65 | loop fusion | bytes 64 | tf_op jit(solution)/shard_map/slice | solution.py:504
  99.4 1.0 slice_bitcast_fusion
  100.4 1.6 %convolution_multiply_fusion = f32[128,128]{1,0:T(8,128)} fusion(bf16[64,128]{1,0:T(8,128)(2,1)} %param.20, bf16[64,128]{1,0:T(8,128)(2,1)S(1)} %copy-done.6, f32[128]{0:T(128)} %bitcast.158), kind=kOutput, calls=%fused_computation.22 | convolution fusion | flops 2179072 | bytes 98816 | tf_op jit(solution)/shard_map/hkt,hks->hts/dot_general | solution.py:515
  101.9 0.9 convolution_multiply_fusion.1
  103.5 1.5 %convolution_bitcast_fusion.2 = f32[64,128]{1,0:T(8,128)} fusion(f32[128,128]{1,0:T(8,128)S(1)} %convolution_multiply_fusion.1, bf16[64,128]{1,0:T(8,128)(2,1)} %param.20), kind=kOutput, calls=%fused_computation.28 | convolution fusion | flops 12582912 | bytes 114688 | tf_op jit(solution)/shard_map/hkt,hts->hks/dot_general | solution.py:518
  105.2 4.0 %fusion.1 = bf16[1,2048,512]{2,1,0:T(8,128)(2,1)} fusion(bf16[8,48,2048]{2,1,0:T(8,128)(2,1)} %get-tuple-element.11, bf16[8,1,48,512]{3,2,0,1:T(8,128)(2,1)S(1)} %get-tuple-element.19), kind=kOutput, calls=%fused_computation.5 | convolution fusion | flops 806354944 | bytes 4063232 | tf_op jit(solution)/shard_map/secd,secf->edf/dot_general | solution.py:474
  110.9 4.2 %fusion = bf16[1,2048,512]{2,1,0:T(8,128)(2,1)} fusion(bf16[8,48,2048]{2,1,0:T(8,128)(2,1)} %get-tuple-element.11, bf16[8,1,48,512]{3,2,0,1:T(8,128)(2,1)} %copy-done.3), kind=kOutput, calls=%fused_computation.4 | convolution fusion | flops 806354944 | bytes 4063232 | tf_op jit(solution)/shard_map/secd,secf->edf/dot_general | solution.py:471
  115.1 2.7 %fusion.2 = bf16[1,512,2048]{2,1,0:T(8,128)(2,1)} fusion(bf16[8,48,2048]{2,1,0:T(8,128)(2,1)S(1)} %copy-done.17, f32[8,1,48,512]{3,2,0,1:T(8,128)S(1)} %copy-done.20, f32[8,1,48,512]{3,2,0,1:T(8,128)S(1)} %copy-done.22), kind=kOutput, calls=%fused_computation.6 | convolution fusion | flops 807534592 | bytes 5242880 | tf_op jit(solution)/shard_map/secf,secd->efd/dot_general | solution.py:468
  119.1 0.9 convolution_add_fusion
  (71 shorter events, 9.2 us)
Async XLA Ops:
  0.6 49.0 %copy-start = (bf16[1,2048,512]{2,1,0:T(8,128)(2,1)S(1)}, bf16[1,2048,512]{2,1,0:T(8,128)(2,1)}, u32[]{:S(2)}) copy-start(bf16[1,2048,512]{2,1,0:T(8,128)(2,1)} %param.25) | copy-start | bytes 6291460
  5.8 49.3 %copy-start.11 = (f32[1,128]{1,0:T(1,128)}, f32[1,128]{1,0:T(1,128)S(1)}, u32[]{:S(2)}) copy-start(f32[1,128]{1,0:T(1,128)S(1)} %fusion.38) | copy-start | bytes 1540
  46.4 3.2 %copy-start.18 = (bf16[8,48,2048]{2,1,0:T(8,128)(2,1)S(1)}, bf16[8,48,2048]{2,1,0:T(8,128)(2,1)}, u32[]{:S(2)}) copy-start(bf16[8,48,2048]{2,1,0:T(8,128)(2,1)} %get-tuple-element.11) | copy-start | bytes 4718596
  49.6 1.0 copy-start.19
  49.6 1.9 %copy-start.15 = (bf16[1,512,2048]{2,1,0:T(8,128)(2,1)S(1)}, bf16[1,512,2048]{2,1,0:T(8,128)(2,1)}, u32[]{:S(2)}) copy-start(bf16[1,512,2048]{2,1,0:T(8,128)(2,1)} %param.27) | copy-start | bytes 6291460
  49.7 2.6 %copy-start.16 = (bf16[8,48,2048]{2,1,0:T(8,128)(2,1)S(1)}, bf16[8,48,2048]{2,1,0:T(8,128)(2,1)}, u32[]{:S(2)}) copy-start(bf16[8,48,2048]{2,1,0:T(8,128)(2,1)} %get-tuple-element.12) | copy-start | bytes 4718596
  50.6 2.8 %copy-start.21 = (f32[8,1,48,512]{3,2,0,1:T(8,128)}, f32[8,1,48,512]{3,2,0,1:T(8,128)S(1)}, u32[]{:S(2)}) copy-start(f32[8,1,48,512]{3,2,0,1:T(8,128)S(1)} %fusion.18) | copy-start | bytes 2359300
  53.5 1.0 copy-start.3
  53.5 2.8 %copy-start.8 = (bf16[64,128]{1,0:T(8,128)(2,1)S(1)}, bf16[64,128]{1,0:T(8,128)(2,1)}, u32[]{:S(2)}) copy-start(bf16[64,128]{1,0:T(8,128)(2,1)} %param.20) | copy-start | bytes 49156
  53.5 2.8 %copy-start.1 = (bf16[1,2048,512]{2,1,0:T(8,128)(2,1)S(1)}, bf16[1,2048,512]{2,1,0:T(8,128)(2,1)}, u32[]{:S(2)}) copy-start(bf16[1,2048,512]{2,1,0:T(8,128)(2,1)} %param.26) | copy-start | bytes 6291460
  58.5 31.1 %copy-start.2 = (bf16[2048,128]{1,0:T(8,128)(2,1)S(1)}, bf16[2048,128]{1,0:T(8,128)(2,1)}, u32[]{:S(2)}) copy-start(bf16[2048,128]{1,0:T(8,128)(2,1)} %param.24) | copy-start | bytes 1572868
  58.5 32.7 %copy-start.10 = (bf16[128,128]{1,0:T(8,128)(2,1)S(1)}, bf16[128,128]{1,0:T(8,128)(2,1)}, u32[]{:S(2)}) copy-start(bf16[128,128]{1,0:T(8,128)(2,1)} %param.19) | copy-start | bytes 98308
  91.3 6.7 %copy-start.12 = (pred[8]{0:T(512)(128)(4,1)}, pred[8]{0:T(512)(128)(4,1)S(1)}, u32[]{:S(2)}) copy-start(pred[8]{0:T(512)(128)(4,1)S(1)} %iota_compare_fusion.5) | copy-start | bytes 28
  91.3 9.1 %copy-start.6 = (bf16[64,128]{1,0:T(8,128)(2,1)S(1)}, bf16[64,128]{1,0:T(8,128)(2,1)}, u32[]{:S(2)}) copy-start(bf16[64,128]{1,0:T(8,128)(2,1)} %keys.1) | copy-start | bytes 49156
  91.3 10.6 %copy-start.4 = (bf16[128,128]{1,0:T(8,128)(2,1)S(1)}, bf16[128,128]{1,0:T(8,128)(2,1)}, u32[]{:S(2)}) copy-start(bf16[128,128]{1,0:T(8,128)(2,1)} %values.1) | copy-start | bytes 98308
  93.7 24.1 %all-to-all-start = ((bf16[8,320,128]{2,1,0:T(8,128)(2,1)}), bf16[8,320,128]{2,1,0:T(8,128)(2,1)S(1)}, u32[]{:S(2)}, u32[]{:S(2)}) async-start(bf16[8,320,128]{2,1,0:T(8,128)(2,1)} %pad_maximum_fusion), calls=%async_computation | async-start | bytes 1310720 | tf_op jit(solution)/shard_map/all_to_all | solution.py:497
  105.1 4.2 %copy-start.13 = (pred[8]{0:T(512)(128)(4,1)S(1)}, pred[8]{0:T(512)(128)(4,1)}, u32[]{:S(2)}) copy-start(pred[8]{0:T(512)(128)(4,1)} %copy-done.12) | copy-start | bytes 28
  105.2 4.1 %copy-start.14 = (f32[8]{0:T(128)S(1)}, f32[8]{0:T(128)}, u32[]{:S(2)}) copy-start(f32[8]{0:T(128)} %slice_reduce_fusion.1) | copy-start | bytes 100
  110.8 4.3 %copy-start.17 = (bf16[8,48,2048]{2,1,0:T(8,128)(2,1)S(1)}, bf16[8,48,2048]{2,1,0:T(8,128)(2,1)}, u32[]{:S(2)}) copy-start(bf16[8,48,2048]{2,1,0:T(8,128)(2,1)} %get-tuple-element.12) | copy-start | bytes 4718596
  110.8 4.3 %copy-start.20 = (f32[8,1,48,512]{3,2,0,1:T(8,128)S(1)}, f32[8,1,48,512]{3,2,0,1:T(8,128)}, u32[]{:S(2)}) copy-start(f32[8,1,48,512]{3,2,0,1:T(8,128)} %copy-done.19) | copy-start | bytes 2359300
  110.9 4.3 %copy-start.22 = (f32[8,1,48,512]{3,2,0,1:T(8,128)S(1)}, f32[8,1,48,512]{3,2,0,1:T(8,128)}, u32[]{:S(2)}) copy-start(f32[8,1,48,512]{3,2,0,1:T(8,128)} %copy-done.21) | copy-start | bytes 2359300
  117.8 1.3 %copy-start.9 = (f32[128,128]{1,0:T(8,128)S(1)}, f32[128,128]{1,0:T(8,128)}, u32[]{:S(2)}) copy-start(f32[128,128]{1,0:T(8,128)} %convolution_multiply_fusion) | copy-start | bytes 196612
  117.8 2.2 %copy-start.5 = (f32[128,128]{1,0:T(8,128)S(1)}, f32[128,128]{1,0:T(8,128)}, u32[]{:S(2)}) copy-start(f32[128,128]{1,0:T(8,128)} %convert_element_type.74) | copy-start | bytes 196612
  117.8 2.2 %copy-start.7 = (f32[64,128]{1,0:T(8,128)S(1)}, f32[64,128]{1,0:T(8,128)}, u32[]{:S(2)}) copy-start(f32[64,128]{1,0:T(8,128)} %convolution_bitcast_fusion.2) | copy-start | bytes 98308
